TPU v7x, 32 devices: a whole 2x2x4 slice. The times are simulated.
32 devices in a mesh: sp: 8 (over z, x), tp: 4 (over y, core).
Axes of the slice: x: 2, y: 2, z: 4, core: 2. Of those that a mesh axis runs over, the one named last changes fastest.
Arguments:
- moe_input: bfloat16 [1536, 2048], P('sp'), may hold values from -6 to 6
- out_grad: bfloat16 [1536, 2048], P('sp', 'tp'), may hold values from -6 to 6
- expert_ids: int32 [1536, 2], P('sp'), may hold values from 0 to 7, all different within a row; in each aligned block of 192 rows (0 to 191, 192 to 383, ...) at most 60 rows name the same one
- expert_weights: float32 [1536, 2], P('sp'), may hold values from 0.1 to 0.9
- w_gate: bfloat16 [8, 2048, 2048], P('sp', None, 'tp'), may hold values from -0.125 to 0.125
- w_up: bfloat16 [8, 2048, 2048], P('sp', None, 'tp'), may hold values from -0.125 to 0.125
- w_down: bfloat16 [8, 2048, 2048], P('sp', 'tp'), may hold values from -0.125 to 0.125
- out_proj: bfloat16 [1536, 2048], P('tp'), may hold values from -0.15625 to 0.15625
- retained: bfloat16 [1536, 1536], P('sp', 'tp'), may hold values from -6 to 6
- queries: bfloat16 [1536, 768], P('sp', 'tp'), may hold values from -6 to 6
- keys: bfloat16 [1536, 768], P('sp', 'tp'), may hold values from -0.86328125 to 0.86328125
- values: bfloat16 [1536, 1536], P('sp', 'tp'), may hold values from -6 to 6
- log_decay: float32 [1536, 16], P('sp', 'tp'), may hold values from -1 to 0
- incoming_state: float32 [8, 16, 48, 96], P('sp', 'tp'), may hold values from -6 to 6
Outputs:
- w_gate_grad: bfloat16 [8, 2048, 2048], P('sp', None, 'tp')
- w_up_grad: bfloat16 [8, 2048, 2048], P('sp', None, 'tp')
- w_down_grad: bfloat16 [8, 2048, 2048], P('sp', 'tp')
- out_proj_grad: float32 [2048, 1536], P('sp', 'tp')
- query_grad: bfloat16 [1536, 768], P('sp', 'tp')
- key_grad: bfloat16 [1536, 768], P('sp', 'tp')
- value_grad: bfloat16 [1536, 1536], P('sp', 'tp')
Inputs may be any that keep to these rules, and one draw needn't show every extreme that they name: `expert_ids`: in each aligned block of 192 positions no expert is named by more than 60 of the block's assignments, a bound that some block reaches.
All inputs are finite; a program needn't handle non-finite values.
Results may differ from a plain program's by a relative error of at most 0.02.
Values may be sent and summed in bfloat16 or wider, within the bound.
A program may use at most 64 MiB of HBM per device.

v0:
```python
import functools

import jax
import jax.numpy as jnp
from jax import lax
from jax.experimental import pallas as pl
from jax.experimental.pallas import tpu as pltpu
from jax.sharding import PartitionSpec as P

MESH = pl.DeviceIdType.MESH
F32 = jnp.float32
BF16 = jnp.bfloat16
LIMIT = 60 * 1024 * 1024


def where_am_i(n, ny):
    s, t = lax.axis_index("sp"), lax.axis_index("tp")
    return s, t, lax.div(t, 2), lax.rem(t, 2)


def greet(peers):
    barrier = pltpu.get_barrier_semaphore()
    for peer in peers:
        pl.semaphore_signal(barrier, inc=1, device_id=peer, device_id_type=MESH)
    pl.semaphore_wait(barrier, len(peers))


def sp_peers(n, s, t):
    return [(lax.rem(s + k, n), t) for k in range(1, n)]


def tp_peers(ny, s, y, c):
    return [(s, lax.rem(y + d, ny) * 2 + c) for d in range(1, ny)] + [(s, y * 2 + 1 - c)]


def remote(src, dst, send, recv, peer):
    return pltpu.make_async_remote_copy(
        src_ref=src, dst_ref=dst, send_sem=send, recv_sem=recv, device_id=peer, device_id_type=MESH
    )


def dispatch_kernel(
    n, ny, cap, route_ref, decay_ref, rows_ref, grad_ref, out_ref, pick_ref, ends_out,
    send_ref, local_sem, a_send, a_recv, e_send, e_recv, y_send, y_recv, p_send, p_recv,
):
    s, t, y, c = where_am_i(n, ny)
    q = grad_ref.shape[1]
    tokens, heads = decay_ref.shape
    partner = (s, y * 2 + 1 - c)

    ids = [route_ref[j : j + 1, :] for j in range(2)]
    weights = [route_ref[j : j + 1, :] for j in range(2, 4)]
    expert = lax.broadcasted_iota(jnp.int32, (n, tokens), 0).astype(F32)
    named = [(expert == own).astype(F32) for own in ids]
    first = lax.broadcasted_iota(jnp.int32, (tokens, tokens), 0)
    second = lax.broadcasted_iota(jnp.int32, (tokens, tokens), 1)
    earlier = jnp.dot(
        (named[0] + named[1]).astype(BF16),
        (first < second).astype(F32).astype(BF16),
        preferred_element_type=F32,
    )
    slot = [
        own * cap + jnp.sum(hot * earlier, axis=0, keepdims=True) for own, hot in zip(ids, named)
    ]
    number = lax.broadcasted_iota(jnp.int32, (n * cap, tokens), 0).astype(F32)
    hits = [(number == own).astype(F32) for own in slot]
    picker = (hits[0] + hits[1]).astype(BF16)
    slot_weight = jnp.sum(hits[0] * weights[0] + hits[1] * weights[1], axis=1, keepdims=True)
    pick_ref[...] = picker
    ends_out[s, :, :] = jnp.zeros((8, 128), F32)
    ends_out[s, :, pl.ds(0, heads)] = jnp.broadcast_to(
        jnp.sum(decay_ref[...], axis=0, keepdims=True), (8, heads)
    )
    own_rows = rows_ref[:, pl.ds(pl.multiple_of(t * q, q), q)]
    picked = jnp.dot(picker, own_rows, preferred_element_type=F32).astype(BF16)
    send_ref[:, 0] = picked.reshape(n, cap, q)
    cotangent = jnp.dot(picker, grad_ref[...], preferred_element_type=F32) * slot_weight
    send_ref[:, 1] = cotangent.astype(BF16).reshape(n, cap, q)

    greet(sp_peers(n, s, t) + tp_peers(ny, s, y, c))

    def block(src, tt):
        rows = pl.ds(pl.multiple_of(src * cap, cap), cap)
        columns = pl.ds(pl.multiple_of(tt * q, q), q)
        return out_ref.at[:, rows, columns]

    own = pltpu.make_async_copy(send_ref.at[s], block(s, t), local_sem.at[0])
    own.start()
    arrivals, waits = [own], []
    for k in range(1, n):
        peer = lax.rem(s + k, n)
        copy = remote(send_ref.at[peer], block(s, t), a_send.at[k], a_recv.at[k], (peer, t))
        copy.start()
        arrivals.append(copy)
        waits.append(copy.wait_send)
    for k in range(1, n):
        peer = lax.rem(s + k, n)
        copy = remote(ends_out.at[s], ends_out.at[s], e_send.at[k], e_recv.at[k], (peer, t))
        copy.start()
        waits.append(copy.wait)
    from_far = {}
    for k in range(n + 1):
        if k < n:
            src = lax.rem(s - k + n, n)
            if k == 0:
                arrivals[0].wait()
            else:
                arrivals[k].wait_recv()
            mine = block(src, t)
            for d in range(1, ny):
                far = (s, lax.rem(y + d, ny) * 2 + c)
                copy = remote(mine, mine, y_send.at[d, k], y_recv.at[d, k], far)
                copy.start()
                waits.append(copy.wait_send)
                from_far[d, k] = copy
            copy = remote(mine, mine, p_send.at[0, k], p_recv.at[0, k], partner)
            copy.start()
            waits.append(copy.wait)
        if k >= 1:
            src = lax.rem(s - k + 1 + n, n)
            for d in range(1, ny):
                from_far[d, k - 1].wait_recv()
                theirs = block(src, lax.rem(y - d + ny, ny) * 2 + c)
                copy = remote(theirs, theirs, p_send.at[d, k - 1], p_recv.at[d, k - 1], partner)
                copy.start()
                waits.append(copy.wait)
    for wait in waits:
        wait()


def dispatch(n, ny, cap, route, decay, rows, grad):
    tokens, q = grad.shape
    dma = pltpu.SemaphoreType.DMA
    return pl.pallas_call(
        functools.partial(dispatch_kernel, n, ny, cap),
        out_shape=(
            jax.ShapeDtypeStruct((2, n * cap, q * ny * 2), BF16),
            jax.ShapeDtypeStruct((n * cap, tokens), BF16),
            jax.ShapeDtypeStruct((n, 8, 128), F32),
        ),
        in_specs=[pl.BlockSpec(memory_space=pltpu.VMEM)] * 4,
        out_specs=[pl.BlockSpec(memory_space=pltpu.VMEM)] * 3,
        scratch_shapes=[pltpu.VMEM((n, 2, cap, q), BF16)]
        + [dma((1,)), dma((n,)), dma((n,)), dma((n,)), dma((n,))]
        + [dma((ny, n))] * 4,
        compiler_params=pltpu.CompilerParams(
            collective_id=0, has_side_effects=True, vmem_limit_bytes=LIMIT
        ),
    )(route, decay, rows, grad)


def combine_kernel(
    n, ny, part_ref, pick_ref, grad_ref, kept_ref, stream_ref, blocks_ref, kept_out,
    near, pairs, far, share, back,
    p_send, p_recv, y_send, y_recv, a_send, a_recv, g_send, g_recv, h_send, h_recv,
    local_sem, r_send, r_recv, l_send, l_recv, x_send, x_recv,
):
    s, t, y, c = where_am_i(n, ny)
    q = grad_ref.shape[1]
    cap = part_ref.shape[0] // n
    greet(sp_peers(n, s, t) + tp_peers(ny, s, y, c))
    partner = (s, y * 2 + 1 - c)
    waits = []

    def columns(tt):
        return pl.ds(pl.multiple_of(tt * q, q), q)

    def rows(b):
        return pl.ds(pl.multiple_of(b * cap, cap), cap)

    nz = n // 2
    z, x = lax.div(s, 2), lax.rem(s, 2)
    pair = (z * 2 + 1 - x, t)
    kept_own = pltpu.make_async_copy(kept_ref, kept_out.at[s], local_sem.at[0])
    kept_own.start()
    waits.append(kept_own.wait)

    def at(zz):
        return lax.rem(zz + 2 * nz, nz) * 2 + x

    def hop(j, sign, send, recv, source):
        held = at(z - sign * j)
        copy = remote(source, kept_out.at[held], send.at[j], recv.at[j], (at(z + sign), t))
        copy.start()
        waits.append(copy.wait_send)
        return copy

    def across(held, index, source):
        copy = remote(source, kept_out.at[held], x_send.at[index], x_recv.at[index], pair)
        copy.start()
        waits.append(copy.wait)

    right_steps, left_steps = nz // 2, nz - 1 - nz // 2
    moving = {}

    def relay(j):
        if j <= right_steps:
            moving["right"].wait_recv()
            held = at(z - j)
            if j < right_steps:
                moving["right"] = hop(j, 1, r_send, r_recv, kept_out.at[held])
            across(held, 2 * j - 1, kept_out.at[held])
        if j <= left_steps:
            moving["left"].wait_recv()
            held = at(z + j)
            if j < left_steps:
                moving["left"] = hop(j, -1, l_send, l_recv, kept_out.at[held])
            across(held, 2 * j, kept_out.at[held])

    halves = {}
    for d in list(range(1, ny)) + [0]:
        theirs = lax.rem(y + d, ny) * 2 + 1 - c
        copy = remote(
            part_ref.at[:, columns(theirs)], near.at[d], p_send.at[d], p_recv.at[d], partner
        )
        copy.start()
        waits.append(copy.wait_send)
        halves[d] = copy
    if right_steps:
        moving["right"] = hop(0, 1, r_send, r_recv, kept_ref)
    if left_steps:
        moving["left"] = hop(0, -1, l_send, l_recv, kept_ref)
    across(s, 0, kept_ref)
    arrived = {}
    for d in range(1, ny):
        halves[d].wait_recv()
        tt = lax.rem(y + d, ny) * 2 + c
        for k in range(1, n + 1):
            b = rows(lax.rem(s + k, n))
            pairs[d, b, :] = (
                part_ref[b, columns(tt)].astype(F32) + near[d, b, :].astype(F32)
            ).astype(BF16)
        for k in range(1, n + 1):
            b = rows(lax.rem(s + k, n))
            copy = remote(
                pairs.at[d, b, :], far.at[d, b, :],
                y_send.at[d, k % n], y_recv.at[d, k % n], (s, tt),
            )
            copy.start()
            waits.append(copy.wait_send)
            arrived[d, k] = copy
    halves[0].wait_recv()
    returns = []
    for k in range(1, n + 1):
        peer = lax.rem(s + k, n)
        b = rows(peer)
        total = part_ref[b, columns(t)].astype(F32) + near[0, b, :].astype(F32)
        for d in range(1, ny):
            arrived[d, k].wait_recv()
            total = total + far[d, b, :].astype(F32)
        if k < n:
            share[b, :] = total.astype(BF16)
            copy = remote(
                share.at[b, :], back.at[rows(s), :], a_send.at[k], a_recv.at[k], (peer, t)
            )
            copy.start()
            waits.append(copy.wait_send)
            returns.append(copy)
        else:
            back[b, :] = total.astype(BF16)
        if k % 2 == 0:
            relay(k // 2)
    for copy in returns:
        copy.wait_recv()
    token = lax.dot_general(
        pick_ref[...], back[...], (((0,), (0,)), ((), ())), preferred_element_type=F32
    )
    stream_ref[:, columns(t)] = (grad_ref[...].astype(F32) + token).astype(BF16)
    mine = stream_ref.at[:, columns(t)]
    outer = []
    for d in range(1, ny):
        copy = remote(
            mine, mine, g_send.at[d], g_recv.at[d], (s, lax.rem(y + d, ny) * 2 + c)
        )
        copy.start()
        waits.append(copy.wait_send)
        outer.append(copy)
    copy = remote(mine, mine, h_send.at[0], h_recv.at[0], partner)
    copy.start()
    waits.append(copy.wait)
    for d in range(1, ny):
        outer[d - 1].wait_recv()
        theirs = stream_ref.at[:, columns(lax.rem(y - d + ny, ny) * 2 + c)]
        copy = remote(theirs, theirs, h_send.at[d], h_recv.at[d], partner)
        copy.start()
        waits.append(copy.wait)
    for wait in waits:
        wait()
    wide = blocks_ref.shape[2]
    for b in range(n):
        blocks_ref[b] = stream_ref[:, b * wide : (b + 1) * wide]


def combine(n, ny, part, pick, grad, kept):
    slots, q = part.shape[0], grad.shape[1]
    dma = pltpu.SemaphoreType.DMA
    return pl.pallas_call(
        functools.partial(combine_kernel, n, ny),
        out_shape=(
            jax.ShapeDtypeStruct((grad.shape[0], q * ny * 2), BF16),
            jax.ShapeDtypeStruct((n, grad.shape[0], q * ny * 2 // n), BF16),
            jax.ShapeDtypeStruct((n,) + kept.shape, BF16),
        ),
        in_specs=[pl.BlockSpec(memory_space=pltpu.VMEM)] * 4,
        out_specs=[pl.BlockSpec(memory_space=pltpu.VMEM)] * 3,
        scratch_shapes=[pltpu.VMEM((ny, slots, q), BF16)] * 3
        + [pltpu.VMEM((slots, q), BF16)] * 2
        + [dma((ny,))] * 2
        + [dma((ny, n))] * 2
        + [dma((n,))] * 2
        + [dma((ny,))] * 4
        + [dma((1,))]
        + [dma((n,))] * 6,
        compiler_params=pltpu.CompilerParams(
            collective_id=1, has_side_effects=True, vmem_limit_bytes=LIMIT
        ),
    )(part, pick, grad, kept)


def tail_kernel(
    n, ny, stream_ref, state_ref, cols_ref, states_ref,
    local_sem, a_send, a_recv, i_send, i_recv, p_send, p_recv,
):
    s, t, y, c = where_am_i(n, ny)
    half = stream_ref.shape[1] // 2
    partner = (s, y * 2 + 1 - c)
    greet(sp_peers(n, s, t) + [partner])
    band = pl.ds(pl.multiple_of(c * half, half), half)
    own = [
        pltpu.make_async_copy(stream_ref.at[s], cols_ref.at[s], local_sem.at[0]),
        pltpu.make_async_copy(state_ref, states_ref.at[s], local_sem.at[1]),
    ]
    for copy in own:
        copy.start()
    waits, arrivals = [copy.wait for copy in own], []
    for k in range(1, n):
        peer = lax.rem(s + k, n)
        copy = remote(state_ref, states_ref.at[s], i_send.at[k], i_recv.at[k], (peer, t))
        copy.start()
        waits.append(copy.wait)
    for k in range(1, n):
        peer = lax.rem(s + k, n)
        copy = remote(
            stream_ref.at[peer, band], cols_ref.at[s, band], a_send.at[k], a_recv.at[k], (peer, t)
        )
        copy.start()
        waits.append(copy.wait_send)
        arrivals.append(copy)
    for k in range(1, n):
        arrivals[k - 1].wait_recv()
        held = cols_ref.at[lax.rem(s - k + n, n), band]
        copy = remote(held, held, p_send.at[k], p_recv.at[k], partner)
        copy.start()
        waits.append(copy.wait)
    for wait in waits:
        wait()


def tail_exchange(n, ny, stream, state):
    dma = pltpu.SemaphoreType.DMA
    return pl.pallas_call(
        functools.partial(tail_kernel, n, ny),
        out_shape=(
            jax.ShapeDtypeStruct(stream.shape, BF16),
            jax.ShapeDtypeStruct((n,) + state.shape, state.dtype),
        ),
        in_specs=[pl.BlockSpec(memory_space=pltpu.VMEM)] * 2,
        out_specs=[pl.BlockSpec(memory_space=pltpu.VMEM)] * 2,
        scratch_shapes=[dma((2,))] + [dma((n,))] * 6,
        compiler_params=pltpu.CompilerParams(
            collective_id=2, has_side_effects=True, vmem_limit_bytes=LIMIT
        ),
    )(stream, state)


def expert_back(rows, grad, gate_w, up_w, down_w):
    f32 = jnp.float32
    bf16 = jnp.bfloat16
    gate = jnp.dot(rows, gate_w, preferred_element_type=f32)
    up = jnp.dot(rows, up_w, preferred_element_type=f32)
    sig = jax.nn.sigmoid(gate)
    swish = gate * sig
    act = (swish * up).astype(bf16)
    across = (((1,), (1,)), ((), ()))
    along = (((0,), (0,)), ((), ()))
    act_grad = lax.dot_general(grad, down_w, across, preferred_element_type=f32)
    gate_grad = (act_grad * up * sig * (1.0 + gate * (1.0 - sig))).astype(bf16)
    up_grad = (act_grad * swish).astype(bf16)
    down_grad = lax.dot_general(act, grad, along, preferred_element_type=f32).astype(bf16)
    gate_w_grad = lax.dot_general(rows, gate_grad, along, preferred_element_type=f32).astype(bf16)
    up_w_grad = lax.dot_general(rows, up_grad, along, preferred_element_type=f32).astype(bf16)
    partial_value = lax.dot_general(
        gate_grad, gate_w, across, preferred_element_type=f32
    ) + lax.dot_general(up_grad, up_w, across, preferred_element_type=f32)
    return (gate_w_grad, up_w_grad, down_grad, partial_value)


def on_device(
    moe_input,
    out_grad,
    expert_ids,
    expert_weights,
    w_gate,
    w_up,
    w_down,
    out_proj,
    retained,
    queries,
    keys,
    values,
    log_decay,
    incoming_state,
):
    f32 = jnp.float32
    bf16 = jnp.bfloat16
    upper_limit = lax.Precision.HIGHEST
    tokens_here = moe_input.shape[0]
    sp_count = lax.axis_size("sp")
    tp_count = lax.axis_size("tp")
    capacity = -(-(5 * tokens_here // (2 * sp_count)) // 16) * 16
    along = (((0,), (0,)), ((), ()))
    ny = tp_count // 2
    heads_here = log_decay.shape[1]
    running_total = jnp.cumsum(log_decay, axis=0)
    last_sum = running_total[-1]
    route = jnp.concatenate([expert_ids.astype(f32).T, expert_weights.T], axis=0)
    received, picker, ends_all = dispatch(
        sp_count, ny, capacity, route, log_decay, moe_input, out_grad
    )
    gate_w_grad, up_w_grad, down_grad, partial_value = expert_back(
        received[0], received[1], w_gate[0], w_up[0], w_down[0]
    )
    stream, stream_blocks, kept_all = combine(
        sp_count, ny, partial_value.astype(bf16), picker, out_grad, retained
    )
    ret_grad = lax.dot_general(
        stream, out_proj, (((1,), (1,)), ((), ())), preferred_element_type=f32
    ).astype(bf16)
    key_dim = queries.shape[1] // heads_here
    value_dim = values.shape[1] // heads_here
    query_rows = queries.astype(f32).reshape(tokens_here, heads_here, key_dim)
    key_matrix = keys.astype(f32).reshape(tokens_here, heads_here, key_dim)
    value_matrix = values.astype(f32).reshape(tokens_here, heads_here, value_dim)
    incoming_gradient = ret_grad.astype(f32).reshape(tokens_here, heads_here, value_dim)
    place = jnp.arange(tokens_here)
    causal = (place[:, None] >= place[None, :])[:, :, None]
    diff = running_total[:, None, :] - running_total[None, :, :]
    decay = jnp.where(causal, jnp.exp(jnp.minimum(diff, 0.0)), 0.0)
    scores = jnp.einsum("thk,shk->tsh", query_rows, key_matrix, precision=upper_limit) * decay
    prob_grad = (
        jnp.einsum("thv,shv->tsh", incoming_gradient, value_matrix, precision=upper_limit) * decay
    )
    added_input = jnp.einsum(
        "yb,ybm,ybx->bmx",
        jnp.exp(running_total),
        query_rows,
        incoming_gradient,
        precision=upper_limit,
    )
    flat_state = added_input.transpose(1, 0, 2).reshape(key_dim, heads_here * value_dim)
    stream_all, states = tail_exchange(sp_count, ny, stream_blocks, flat_state.astype(bf16))
    out_proj_grad = lax.dot_general(
        stream_all.reshape(sp_count * tokens_here, -1),
        kept_all.reshape(sp_count * tokens_here, -1),
        along,
        preferred_element_type=f32,
    )
    block_ends = ends_all[:, 0, :heads_here]
    before = jnp.cumsum(block_ends, axis=0) - block_ends
    here = lax.axis_index("sp")
    since = jnp.sum(
        jnp.where(jnp.arange(sp_count)[:, None] <= here, block_ends, 0.0), axis=0, keepdims=True
    )
    reach = jnp.where(
        jnp.arange(sp_count)[:, None] > here, jnp.exp(jnp.minimum(before - since, 0.0)), 0.0
    )
    state_gradient = jnp.sum(
        states.astype(f32).reshape(sp_count, key_dim, heads_here, value_dim)
        * reach[:, None, :, None],
        axis=0,
    ).transpose(1, 0, 2)
    tail = jnp.exp(last_sum[None, :] - running_total)[..., None]
    query_grad = jnp.einsum("tsh,shk->thk", prob_grad, key_matrix, precision=upper_limit) + jnp.exp(
        running_total
    )[..., None] * jnp.einsum(
        "ybc,bfc->ybf", incoming_gradient, incoming_state[0], precision=upper_limit
    )
    key_grad = jnp.einsum(
        "tsh,thk->shk", prob_grad, query_rows, precision=upper_limit
    ) + tail * jnp.einsum("rgd,gnd->rgn", value_matrix, state_gradient, precision=upper_limit)
    value_grad = jnp.einsum(
        "tsh,thv->shv", scores, incoming_gradient, precision=upper_limit
    ) + tail * jnp.einsum("bgi,gie->bge", key_matrix, state_gradient, precision=upper_limit)
    return (
        gate_w_grad[None],
        up_w_grad[None],
        down_grad[None],
        out_proj_grad,
        query_grad.reshape(tokens_here, -1).astype(bf16),
        key_grad.reshape(tokens_here, -1).astype(bf16),
        value_grad.reshape(tokens_here, -1).astype(bf16),
    )


def solution(mesh):
    placed = (
        P("sp", None),
        P("sp", "tp"),
        P("sp", None),
        P("sp", None),
        P("sp", None, "tp"),
        P("sp", None, "tp"),
        P("sp", "tp", None),
        P("tp", None),
        P("sp", "tp"),
        P("sp", "tp"),
        P("sp", "tp"),
        P("sp", "tp"),
        P("sp", "tp"),
        P("sp", "tp", None, None),
    )
    return jax.shard_map(
        on_device,
        mesh=mesh,
        in_specs=placed,
        out_specs=(
            P("sp", None, "tp"),
            P("sp", None, "tp"),
            P("sp", "tp", None),
            P("sp", "tp"),
            P("sp", "tp"),
            P("sp", "tp"),
            P("sp", "tp"),
        ),
        check_vma=False,
    )
```

profile of v0, /device:TPU:0, one launch (start us, length us, event | category | flops | bytes accessed | tf_op | source)
XLA Modules:
  0.0 150.3 jit_solution(13631144776751140248)
XLA Ops:
  0.6 1.6 %copy.90.decay_ref = f32[192,4]{1,0:T(8,128)} copy(f32[192,4]{0,1:T(4,128)} %param.26) | data formatting | bytes 6144 | tf_op args[12]
  2.2 0.7 convert_bitcast_fusion
  2.9 1.3 pad_maximum_fusion.route_ref
  4.2 43.0 %shard_map.189 = (bf16[2,512,2048]{2,1,0:T(8,128)(2,1)}, bf16[512,192]{1,0:T(8,128)(2,1)}, f32[8,8,128]{2,1,0:T(8,128)}) custom-call(f32[4,192]{1,0:T(4,128)} %pad_maximum_fusion.route_ref, f32[192,4]{1,0:T(8,128)} %copy.90.decay_ref, bf16[192,2048]{1,0:T(8,128)(2,1)} %rows_ref.1, bf16[192,512]{1,0:T(8,128)(2,1)} %grad_ref.3), custom_call_target="tpu_custom_call" | custom-call | tf_op jit(solution)/shard_map/pallas_call | solution.py:134
  47.3 3.0 %fusion.5 = f32[512,512]{1,0:T(8,128)S(1)} fusion(bf16[1,2048,512]{2,1,0:T(8,128)(2,1)S(1)} %copy-done, bf16[2,512,2048]{2,1,0:T(8,128)(2,1)} %get-tuple-element.15), kind=kOutput, calls=%fused_computation.9 | convolution fusion | flops 1073741824 | bytes 5242880 | tf_op jit(solution)/shard_map/dot_general | solution.py:379
  50.3 0.4 copy-done.11
  50.7 1.2 fusion.8
  52.0 0.7 copy-done.13
  52.7 1.6 %multiply_convert_fusion.1 = (bf16[512,512]{1,0:T(8,128)(2,1)S(1)}, bf16[512,512]{1,0:T(8,128)(2,1)S(1)}) fusion(f32[512,512]{1,0:T(8,128)S(1)} %fusion.5, f32[512,512]{1,0:T(8,128)S(1)} %fusion.8, bf16[1,512,2048]{2,1,0:T(8,128)(2,1)S(1)} %copy-done.13, bf16[2,512,2048]{2,1,0:T(8,128)(2,1)S(1)} %copy-done.11), kind=kOutput, calls=%fused_computation.52 | convolution fusion | flops 1077149696 | bytes 7340032 | tf_op jit(solution)/shard_map/dot_general | solution.py:386
  54.3 1.3 fusion.3
  55.7 2.6 %add_convert_fusion.part_ref = bf16[512,2048]{1,0:T(8,128)(2,1)} fusion(f32[512,2048]{1,0:T(8,128)S(1)} %fusion.3, bf16[512,512]{1,0:T(8,128)(2,1)S(1)} %get-tuple-element.51, bf16[1,2048,512]{2,1,0:T(8,128)(2,1)S(1)} %copy-done.1), kind=kOutput, calls=%fused_computation | convolution fusion | flops 1075838976 | bytes 8912896 | tf_op jit(solution)/shard_map/dot_general | solution.py:394
  58.3 43.5 %shard_map.190 = (bf16[192,2048]{1,0:T(8,128)(2,1)}, bf16[8,192,256]{2,1,0:T(8,128)(2,1)}, bf16[8,192,384]{2,1,0:T(8,128)(2,1)}) custom-call(bf16[512,2048]{1,0:T(8,128)(2,1)} %add_convert_fusion.part_ref, bf16[512,192]{1,0:T(8,128)(2,1)} %get-tuple-element.16.pick_ref, bf16[192,512]{1,0:T(8,128)(2,1)} %grad_ref.3, bf16[192,384]{1,0:T(8,128)(2,1)} %kept_ref.1), custom_call_target="tpu_custom_call" | custom-call | tf_op jit(solution)/shard_map/pallas_call | solution.py:297
  101.9 1.8 %convolution_convert_fusion.3 = bf16[192,384]{1,0:T(8,128)(2,1)S(1)} fusion(bf16[192,2048]{1,0:T(8,128)(2,1)} %get-tuple-element.18, bf16[384,2048]{1,0:T(8,128)(2,1)S(1)} %copy-done.2), kind=kOutput, calls=%fused_computation.38 | convolution fusion | flops 302063616 | bytes 2506752 | tf_op jit(solution)/shard_map/dot_general | solution.py:436
  103.7 0.1 copy.111
  103.9 1.2 reduce-window.6
  105.1 0.1 slice.29
  105.2 0.1 copy.91
  105.3 0.1 copy.92
  105.5 0.2 slice_reduce_fusion
  105.8 0.1 copy.93
  105.9 0.3 fusion.35
  106.2 0.7 convert_element_type.70.state_ref
  107.0 21.4 %shard_map.191 = (bf16[8,192,256]{2,1,0:T(8,128)(2,1)}, bf16[8,48,384]{2,1,0:T(8,128)(2,1)}) custom-call(bf16[8,192,256]{2,1,0:T(8,128)(2,1)} %get-tuple-element.17.stream_ref, bf16[48,384]{1,0:T(8,128)(2,1)} %convert_element_type.70.state_ref), custom_call_target="tpu_custom_call" | custom-call | tf_op jit(solution)/shard_map/pallas_call | solution.py:361
  128.3 0.8 slice.28
  129.1 0.1 copy.100
  129.2 0.1 select_reduce_fusion
  129.3 0.2 reduce_window_sum.31
  129.6 0.1 copy.101
  129.7 0.1 mul.73
  129.8 1.0 multiply_reduce_fusion
  130.9 0.1 reduce_sum.22
  131.0 0.1 copy.98
  131.1 0.4 fusion.24
  131.5 0.4 convolution_bitcast_fusion.4
  131.9 0.4 fusion.28
  132.3 0.8 copy.109
  133.1 0.1 reshape.120
  133.3 0.5 fusion.31
  133.7 0.4 fusion.25
  134.1 0.4 fusion.34
  134.5 0.7 copy.108
  135.3 1.1 fusion.32
  136.4 0.5 fusion.33
  137.0 0.7 copy.107
  137.7 2.9 %convolution_bitcast_fusion.2 = f32[256,384]{1,0:T(8,128)} fusion(bf16[8,192,256]{2,1,0:T(8,128)(2,1)} %get-tuple-element.19, bf16[8,192,384]{2,1,0:T(8,128)(2,1)} %get-tuple-element.20), kind=kOutput, calls=%fused_computation.32 | convolution fusion | flops 301989888 | bytes 2359296 | tf_op jit(solution)/shard_map/dot_general | solution.py:462
  140.6 4.4 %fusion.1 = bf16[1,2048,512]{2,1,0:T(8,128)(2,1)} fusion(bf16[512,512]{1,0:T(8,128)(2,1)S(1)} %copy-done.6, bf16[2,512,2048]{2,1,0:T(8,128)(2,1)} %get-tuple-element.15), kind=kOutput, calls=%fused_computation.5 | convolution fusion | flops 1074790400 | bytes 4718592 | tf_op jit(solution)/shard_map/dot_general | solution.py:391
  144.9 2.6 %fusion = bf16[1,2048,512]{2,1,0:T(8,128)(2,1)} fusion(bf16[512,512]{1,0:T(8,128)(2,1)S(1)} %copy-done.4, bf16[2,512,2048]{2,1,0:T(8,128)(2,1)S(1)} %copy-done.12), kind=kOutput, calls=%fused_computation.4 | convolution fusion | flops 1074790400 | bytes 4718592 | tf_op jit(solution)/shard_map/dot_general | solution.py:390
  147.6 2.7 %fusion.2 = bf16[1,512,2048]{2,1,0:T(8,128)(2,1)} fusion(bf16[2,512,2048]{2,1,0:T(8,128)(2,1)S(1)} %copy-done.12, f32[512,512]{1,0:T(8,128)S(1)} %copy-done.17, f32[512,512]{1,0:T(8,128)S(1)} %copy-done.15), kind=kOutput, calls=%fused_computation.6 | convolution fusion | flops 1076363264 | bytes 6291456 | tf_op jit(solution)/shard_map/dot_general | solution.py:389
  (46 shorter events, 0.5 us)
Async XLA Ops:
  0.6 46.6 %copy-start = (bf16[1,2048,512]{2,1,0:T(8,128)(2,1)S(1)}, bf16[1,2048,512]{2,1,0:T(8,128)(2,1)}, u32[]{:S(2)}) copy-start(bf16[1,2048,512]{2,1,0:T(8,128)(2,1)} %param.18) | copy-start | bytes 6291460
  47.3 3.0 %copy-start.1 = (bf16[1,2048,512]{2,1,0:T(8,128)(2,1)S(1)}, bf16[1,2048,512]{2,1,0:T(8,128)(2,1)}, u32[]{:S(2)}) copy-start(bf16[1,2048,512]{2,1,0:T(8,128)(2,1)} %param.19) | copy-start | bytes 6291460
  47.3 3.4 %copy-start.11 = (bf16[2,512,2048]{2,1,0:T(8,128)(2,1)S(1)}, bf16[2,512,2048]{2,1,0:T(8,128)(2,1)}, u32[]{:S(2)}) copy-start(bf16[2,512,2048]{2,1,0:T(8,128)(2,1)} %get-tuple-element.15) | copy-start | bytes 12582916
  50.7 1.3 copy-start.14
  50.7 2.0 %copy-start.13 = (bf16[1,512,2048]{2,1,0:T(8,128)(2,1)S(1)}, bf16[1,512,2048]{2,1,0:T(8,128)(2,1)}, u32[]{:S(2)}) copy-start(bf16[1,512,2048]{2,1,0:T(8,128)(2,1)} %param.20) | copy-start | bytes 6291460
  52.7 1.6 %copy-start.16 = (f32[512,512]{1,0:T(8,128)}, f32[512,512]{1,0:T(8,128)S(1)}, u32[]{:S(2)}) copy-start(f32[512,512]{1,0:T(8,128)S(1)} %fusion.8) | copy-start | bytes 3145732
  54.3 1.3 copy-start.3
  54.3 1.3 copy-start.5
  58.3 43.6 %copy-start.2 = (bf16[384,2048]{1,0:T(8,128)(2,1)S(1)}, bf16[384,2048]{1,0:T(8,128)(2,1)}, u32[]{:S(2)}) copy-start(bf16[384,2048]{1,0:T(8,128)(2,1)} %param.21) | copy-start | bytes 4718596
  101.8 2.0 %copy-start.10 = (f32[192,4]{0,1:T(4,128)S(1)}, f32[192,4]{0,1:T(4,128)}, u32[]{:S(2)}) copy-start(f32[192,4]{0,1:T(4,128)} %param.26) | copy-start | bytes 9220
  101.8 4.0 %copy-start.8 = (bf16[192,192]{1,0:T(8,128)(2,1)S(1)}, bf16[192,192]{1,0:T(8,128)(2,1)}, u32[]{:S(2)}) copy-start(bf16[192,192]{1,0:T(8,128)(2,1)} %param.23) | copy-start | bytes 221188
  101.8 29.1 %copy-start.9 = (bf16[192,192]{1,0:T(8,128)(2,1)S(1)}, bf16[192,192]{1,0:T(8,128)(2,1)}, u32[]{:S(2)}) copy-start(bf16[192,192]{1,0:T(8,128)(2,1)} %param.24) | copy-start | bytes 221188
  131.0 2.1 %copy-start.7 = (bf16[192,384]{1,0:T(8,128)(2,1)S(1)}, bf16[192,384]{1,0:T(8,128)(2,1)}, u32[]{:S(2)}) copy-start(bf16[192,384]{1,0:T(8,128)(2,1)} %param.25) | copy-start | bytes 442372
  136.9 3.6 %copy-start.6 = (bf16[512,512]{1,0:T(8,128)(2,1)S(1)}, bf16[512,512]{1,0:T(8,128)(2,1)}, u32[]{:S(2)}) copy-start(bf16[512,512]{1,0:T(8,128)(2,1)} %copy-done.5) | copy-start | bytes 1572868
  140.6 4.4 %copy-start.4 = (bf16[512,512]{1,0:T(8,128)(2,1)S(1)}, bf16[512,512]{1,0:T(8,128)(2,1)}, u32[]{:S(2)}) copy-start(bf16[512,512]{1,0:T(8,128)(2,1)} %copy-done.3) | copy-start | bytes 1572868
  140.6 4.4 %copy-start.12 = (bf16[2,512,2048]{2,1,0:T(8,128)(2,1)S(1)}, bf16[2,512,2048]{2,1,0:T(8,128)(2,1)}, u32[]{:S(2)}) copy-start(bf16[2,512,2048]{2,1,0:T(8,128)(2,1)} %get-tuple-element.15) | copy-start | bytes 12582916
  144.9 2.7 %copy-start.15 = (f32[512,512]{1,0:T(8,128)S(1)}, f32[512,512]{1,0:T(8,128)}, u32[]{:S(2)}) copy-start(f32[512,512]{1,0:T(8,128)} %copy-done.14) | copy-start | bytes 3145732
  144.9 2.7 %copy-start.17 = (f32[512,512]{1,0:T(8,128)S(1)}, f32[512,512]{1,0:T(8,128)}, u32[]{:S(2)}) copy-start(f32[512,512]{1,0:T(8,128)} %copy-done.16) | copy-start | bytes 3145732
where the time goes:
time: 151 us; the launch traced here: 150 us
  Pallas kernels  108 us (72%)
  matrix products  28.5 us (19%)
  local copies, waits for them, and re-layouts  8.04 us (5%)
  other arithmetic  4.81 us (3%)
    pallas_call x1, Pallas kernels, combine(): pl.pallas_call(functools.partial(combine_kernel, n, ny), out_shape=(jax.S...  43.5 us
    pallas_call x1, Pallas kernels, dispatch(): pl.pallas_call(functools.partial(dispatch_kernel, n, ny, cap), out_shape=...  43 us
    pallas_call x1, Pallas kernels, tail_exchange(): pl.pallas_call(functools.partial(tail_kernel, n, ny), out_shape=(jax.Shap...  21.4 us
    unnamed x43, local copies, waits for them, and re-layouts  5.33 us
    dot_general x1, matrix products, expert_back(): lax.dot_general(rows, up_grad, along, preferred_element_type=f32)  4.35 us

commit v1 on v0

v1 whole, which is shorter than its diff:
```python
import functools

import jax
import jax.numpy as jnp
from jax import lax
from jax.experimental import pallas as pl
from jax.experimental.pallas import tpu as pltpu
from jax.sharding import PartitionSpec as P

MESH = pl.DeviceIdType.MESH
F32 = jnp.float32
BF16 = jnp.bfloat16
LIMIT = 60 * 1024 * 1024


def where_am_i(n, ny):
    s, t = lax.axis_index("sp"), lax.axis_index("tp")
    return s, t, lax.div(t, 2), lax.rem(t, 2)


def greet(peers):
    barrier = pltpu.get_barrier_semaphore()
    for peer in peers:
        pl.semaphore_signal(barrier, inc=1, device_id=peer, device_id_type=MESH)
    pl.semaphore_wait(barrier, len(peers))


def sp_peers(n, s, t):
    return [(lax.rem(s + k, n), t) for k in range(1, n)]


def tp_peers(ny, s, y, c):
    return [(s, lax.rem(y + d, ny) * 2 + c) for d in range(1, ny)] + [(s, y * 2 + 1 - c)]


def remote(src, dst, send, recv, peer):
    return pltpu.make_async_remote_copy(
        src_ref=src, dst_ref=dst, send_sem=send, recv_sem=recv, device_id=peer, device_id_type=MESH
    )


def below(a, b, top):
    return lax.div(b - a + top - 1, top)


def nearest_first(z, nz):
    high = nz - 1 - z
    fewer = below(high, z, nz)
    least = z + (high - z) * fewer
    toward = 1 - 2 * fewer
    order = [z]
    for i in range(1, nz):
        both = below(i, 2 * least + 1, 2 * nz)
        step = (i + 1) // 2 * (1 if i % 2 else -1)
        order.append(z + toward * (both * step + (1 - both) * (i - least)))
    return order


def main_kernel(
    n, ny, cap, ids_ref, weights_ref, decay_ref, rows_hbm, grad_ref, kept_ref,
    gate_hbm, up_hbm, down_hbm,
    stream_ref, blocks_ref, kept_out, ends_out, gate_grad_ref, up_grad_ref, down_grad_ref,
    rows_v, gate_w, up_w, down_w, pick, send, slots, act, both_grads, part, near, pairs, far,
    share, back,
    load_sem, a_send, a_recv, e_send, e_recv, y_send, y_recv, p_send, p_recv,
    n_send, n_recv, f_send, f_recv, b_send, b_recv, g_send, g_recv, h_send, h_recv,
    r_send, r_recv, l_send, l_recv, x_send, x_recv,
):
    s, t, y, c = where_am_i(n, ny)
    q = grad_ref.shape[1]
    heads, tokens = decay_ref.shape
    width = gate_w.shape[1]
    nz = n // 2
    z, x = lax.div(s, 2), lax.rem(s, 2)
    partner = (s, y * 2 + 1 - c)
    order = nearest_first(z, nz)
    waits = []

    def columns(tt):
        return pl.ds(pl.multiple_of(tt * q, q), q)

    def block_rows(b):
        return pl.ds(pl.multiple_of(b * cap, cap), cap)

    def chunk_rows(i):
        return pl.ds(pl.multiple_of(order[i] * 2 * cap, 2 * cap), 2 * cap)

    def member(i, e):
        return order[i] * 2 + (x if e == 0 else 1 - x)

    def away(d):
        return (s, lax.rem(y + d, ny) * 2 + c)

    def go(copy, wait):
        copy.start()
        waits.append(getattr(copy, wait))
        return copy

    barrier = pltpu.get_barrier_semaphore()
    peers = sp_peers(n, s, t) + tp_peers(ny, s, y, c)
    for peer in peers:
        pl.semaphore_signal(barrier, inc=1, device_id=peer, device_id_type=MESH)

    own_rows = pltpu.make_async_copy(rows_hbm.at[:, columns(t)], rows_v, load_sem.at[0])
    own_rows.start()
    loads = [
        pltpu.make_async_copy(hbm, local, load_sem.at[1 + j])
        for j, (hbm, local) in enumerate(
            [(gate_hbm.at[0], gate_w), (up_hbm.at[0], up_w), (down_hbm.at[0], down_w)]
        )
    ]
    for copy in loads:
        copy.start()

    ids = ids_ref[...].astype(F32)
    ids = [ids[j : j + 1, :] for j in range(2)]
    weights = [weights_ref[j : j + 1, :] for j in range(2)]
    expert_row = lax.broadcasted_iota(jnp.int32, (n, tokens), 0).astype(F32)
    named = [(expert_row == own).astype(F32) for own in ids]
    first = lax.broadcasted_iota(jnp.int32, (tokens, tokens), 0)
    second = lax.broadcasted_iota(jnp.int32, (tokens, tokens), 1)
    earlier = jnp.dot(
        (named[0] + named[1]).astype(BF16),
        (first < second).astype(F32).astype(BF16),
        preferred_element_type=F32,
    )
    slot = [
        own * cap + jnp.sum(hot * earlier, axis=0, keepdims=True) for own, hot in zip(ids, named)
    ]
    number = lax.broadcasted_iota(jnp.int32, (n * cap, tokens), 0).astype(F32)
    hits = [(number == own).astype(F32) for own in slot]
    picker = (hits[0] + hits[1]).astype(BF16)
    slot_weight = jnp.sum(hits[0] * weights[0] + hits[1] * weights[1], axis=1, keepdims=True)
    pick[...] = picker
    ends_out[s, :, :] = jnp.zeros((8, 128), F32)
    ends_out[s, pl.ds(0, heads), :] = jnp.broadcast_to(
        jnp.sum(decay_ref[...], axis=1, keepdims=True), (heads, 128)
    )
    cotangent = jnp.dot(picker, grad_ref[...], preferred_element_type=F32) * slot_weight
    send[:, 1] = cotangent.astype(BF16).reshape(n, cap, q)
    own_rows.wait()
    picked = jnp.dot(picker, rows_v[...], preferred_element_type=F32).astype(BF16)
    send[:, 0] = picked.reshape(n, cap, q)
    slots[0, block_rows(s), columns(t)] = send[s, 0]
    slots[1, block_rows(s), columns(t)] = send[s, 1]

    pl.semaphore_wait(barrier, len(peers))

    def block(src, tt):
        return slots.at[:, block_rows(src), columns(tt)]

    for i in range(nz):
        for e in range(2):
            if (i, e) != (0, 0):
                to = member(i, e)
                go(
                    remote(send.at[to], block(s, t), a_send.at[2 * i + e], a_recv.at[s], (to, t)),
                    "wait_send",
                )

    def at(zz):
        return lax.rem(zz + 2 * nz, nz) * 2 + x

    def hop(j, sign, send_sem, recv_sem, source):
        held = at(z - sign * j)
        return go(
            remote(
                source, kept_out.at[held], send_sem.at[j], recv_sem.at[j], (at(z + sign), t)
            ),
            "wait_send",
        )

    def across(held, index, source):
        go(
            remote(
                source, kept_out.at[held], x_send.at[index], x_recv.at[index],
                (z * 2 + 1 - x, t),
            ),
            "wait",
        )

    right_steps, left_steps = nz // 2, nz - 1 - nz // 2
    moving = {}

    def kept_start():
        if right_steps:
            moving["right"] = hop(0, 1, r_send, r_recv, kept_ref)
        if left_steps:
            moving["left"] = hop(0, -1, l_send, l_recv, kept_ref)
        across(s, 0, kept_ref)
        kept_out[s] = kept_ref[...]

    def kept_relay(j):
        if j <= right_steps:
            moving["right"].wait_recv()
            held = at(z - j)
            if j < right_steps:
                moving["right"] = hop(j, 1, r_send, r_recv, kept_out.at[held])
            across(held, 2 * j - 1, kept_out.at[held])
        if j <= left_steps:
            moving["left"].wait_recv()
            held = at(z + j)
            if j < left_steps:
                moving["left"] = hop(j, -1, l_send, l_recv, kept_out.at[held])
            across(held, 2 * j, kept_out.at[held])

    from_far, from_partner = {}, {}

    def arrive(i, e):
        src = member(i, e)
        mine = block(src, t)
        if (i, e) != (0, 0):
            remote(
                send.at[src], mine, a_send.at[2 * i + e], a_recv.at[src], (src, t)
            ).wait_recv()
        k = 2 * i + e
        for d in range(1, ny):
            from_far[d, k] = go(
                remote(mine, mine, y_send.at[d, k], y_recv.at[d, k], away(d)), "wait_send"
            )
        from_partner[0, k] = go(
            remote(mine, mine, p_send.at[0, k], p_recv.at[0, k], partner), "wait_send"
        )

    def relay(i, e):
        k = 2 * i + e
        for d in range(1, ny):
            from_far[d, k].wait_recv()
            theirs = block(member(i, e), lax.rem(y - d + ny, ny) * 2 + c)
            from_partner[d, k] = go(
                remote(theirs, theirs, p_send.at[d, k], p_recv.at[d, k], partner), "wait_send"
            )

    across_dims = (((1,), (1,)), ((), ()))
    along_dims = (((0,), (0,)), ((), ()))

    def expert(i):
        for e in range(2):
            for d in range(ny):
                from_partner[d, 2 * i + e].wait_recv()
        r = chunk_rows(i)
        gate = jnp.dot(slots[0, r, :], gate_w[...], preferred_element_type=F32)
        up = jnp.dot(slots[0, r, :], up_w[...], preferred_element_type=F32)
        act_grad = lax.dot_general(
            slots[1, r, :], down_w[...], across_dims, preferred_element_type=F32
        )
        sig = jax.nn.sigmoid(gate)
        swish = gate * sig
        act[r, :] = (swish * up).astype(BF16)
        gate_grad = (act_grad * up * sig * (1.0 + gate * (1.0 - sig))).astype(BF16)
        up_grad = (act_grad * swish).astype(BF16)
        both_grads[r, pl.ds(0, width)] = gate_grad
        both_grads[r, pl.ds(width, width)] = up_grad
        part[r, :] = (
            lax.dot_general(gate_grad, gate_w[...], across_dims, preferred_element_type=F32)
            + lax.dot_general(up_grad, up_w[...], across_dims, preferred_element_type=F32)
        ).astype(BF16)

    halves, summed, returns = {}, {}, {}

    def swap_halves(i):
        r = chunk_rows(i)
        for d in list(range(1, ny)) + [0]:
            theirs = lax.rem(y + d, ny) * 2 + 1 - c
            halves[d, i] = go(
                remote(
                    part.at[r, columns(theirs)], near.at[d, r, :],
                    n_send.at[d, i], n_recv.at[d, i], partner,
                ),
                "wait_send",
            )

    def send_pairs(i):
        r = chunk_rows(i)
        for d in range(1, ny):
            halves[d, i].wait_recv()
            tt = lax.rem(y + d, ny) * 2 + c
            pairs[d, r, :] = (
                part[r, columns(tt)].astype(F32) + near[d, r, :].astype(F32)
            ).astype(BF16)
            summed[d, i] = go(
                remote(
                    pairs.at[d, r, :], far.at[d, r, :], f_send.at[d, i], f_recv.at[d, i], (s, tt)
                ),
                "wait_send",
            )

    def send_back(i):
        r = chunk_rows(i)
        halves[0, i].wait_recv()
        total = part[r, columns(t)].astype(F32) + near[0, r, :].astype(F32)
        for d in range(1, ny):
            summed[d, i].wait_recv()
            total = total + far[d, r, :].astype(F32)
        share[r, :] = total.astype(BF16)
        for e in range(2):
            to = member(i, e)
            if (i, e) == (0, 0):
                back[block_rows(s), :] = share[block_rows(s), :]
            else:
                go(
                    remote(
                        share.at[block_rows(to), :], back.at[block_rows(s), :],
                        b_send.at[2 * i + e], b_recv.at[s], (to, t),
                    ),
                    "wait_send",
                )

    def returned(i):
        for e in range(2):
            if (i, e) != (0, 0):
                src = member(i, e)
                remote(
                    share.at[block_rows(src), :], back.at[block_rows(src), :],
                    b_send.at[2 * i + e], b_recv.at[src], (src, t),
                ).wait_recv()
        r = chunk_rows(i)
        return lax.dot_general(
            pick[r, :], back[r, :], along_dims, preferred_element_type=F32
        )

    def down_grads():
        turned = act[...].T
        wide = 512
        for j in range(0, down_grad_ref.shape[2], wide):
            down_grad_ref[0, :, j : j + wide] = jnp.dot(
                turned, slots[1, :, j : j + wide], preferred_element_type=F32
            ).astype(BF16)

    def in_grads(lo, hi):
        tall = 256

        def step(j, carry):
            band = pl.ds(pl.multiple_of(j * tall, tall), tall)
            grads = lax.dot_general(
                slots[0, :, band], both_grads[...], along_dims, preferred_element_type=F32
            ).astype(BF16)
            gate_grad_ref[0, band, :] = grads[:, :width]
            up_grad_ref[0, band, :] = grads[:, width:]
            return carry

        count = gate_grad_ref.shape[1] // tall
        lax.fori_loop(lo * count // 4, hi * count // 4, step, 0)

    for k in range(1, n):
        to = lax.rem(s + k, n)
        go(remote(ends_out.at[s], ends_out.at[s], e_send.at[k], e_recv.at[k], (to, t)), "wait")
    kept_start()
    for i in range(nz + 1):
        if i < nz:
            arrive(i, 0)
            arrive(i, 1)
        if i == 1:
            for copy in loads:
                copy.wait()
        if i >= 1:
            relay(i - 1, 0)
            relay(i - 1, 1)
        if i >= 2:
            send_pairs(i - 2)
        if i >= 3:
            send_back(i - 3)
        if i >= 1:
            expert(i - 1)
            swap_halves(i - 1)
        if i >= 2:
            kept_relay(i - 1)
    send_back(nz - 2) if nz > 1 else None
    send_pairs(nz - 1)
    down_grads()
    send_back(nz - 1)
    in_grads(0, 2)
    token = returned(0)
    for i in range(1, nz):
        token = token + returned(i)
    stream_ref[:, columns(t)] = (grad_ref[...].astype(F32) + token).astype(BF16)
    mine = stream_ref.at[:, columns(t)]
    outer = {}
    for d in range(1, ny):
        outer[d] = go(remote(mine, mine, g_send.at[d], g_recv.at[d], away(d)), "wait_send")
    go(remote(mine, mine, h_send.at[0], h_recv.at[0], partner), "wait")
    in_grads(2, 4)
    for d in range(1, ny):
        outer[d].wait_recv()
        theirs = stream_ref.at[:, columns(lax.rem(y - d + ny, ny) * 2 + c)]
        go(remote(theirs, theirs, h_send.at[d], h_recv.at[d], partner), "wait")
    for wait in waits:
        wait()
    wide = blocks_ref.shape[2]
    for b in range(n):
        blocks_ref[b] = stream_ref[:, b * wide : (b + 1) * wide]


def main_part(n, ny, cap, ids, weights, decay, rows, grad, kept, gate_w, up_w, down_w):
    tokens, q = grad.shape
    dma = pltpu.SemaphoreType.DMA
    slots, model, width = n * cap, rows.shape[1], gate_w.shape[2]
    nz = n // 2
    vmem, anywhere = pl.BlockSpec(memory_space=pltpu.VMEM), pl.BlockSpec(memory_space=pl.ANY)
    return pl.pallas_call(
        functools.partial(main_kernel, n, ny, cap),
        out_shape=(
            jax.ShapeDtypeStruct((tokens, model), BF16),
            jax.ShapeDtypeStruct((n, tokens, model // n), BF16),
            jax.ShapeDtypeStruct((n,) + kept.shape, BF16),
            jax.ShapeDtypeStruct((n, 8, 128), F32),
            jax.ShapeDtypeStruct(gate_w.shape, BF16),
            jax.ShapeDtypeStruct(up_w.shape, BF16),
            jax.ShapeDtypeStruct(down_w.shape, BF16),
        ),
        in_specs=[vmem, vmem, vmem, anywhere, vmem, vmem, anywhere, anywhere, anywhere],
        out_specs=[vmem] * 7,
        scratch_shapes=[
            pltpu.VMEM((tokens, q), BF16),
            pltpu.VMEM(gate_w.shape[1:], BF16),
            pltpu.VMEM(up_w.shape[1:], BF16),
            pltpu.VMEM(down_w.shape[1:], BF16),
            pltpu.VMEM((slots, tokens), BF16),
            pltpu.VMEM((n, 2, cap, q), BF16),
            pltpu.VMEM((2, slots, model), BF16),
            pltpu.VMEM((slots, width), BF16),
            pltpu.VMEM((slots, 2 * width), BF16),
            pltpu.VMEM((slots, model), BF16),
            pltpu.VMEM((ny, slots, q), BF16),
            pltpu.VMEM((ny, slots, q), BF16),
            pltpu.VMEM((ny, slots, q), BF16),
            pltpu.VMEM((slots, q), BF16),
            pltpu.VMEM((slots, q), BF16),
            dma((4,)),
        ]
        + [dma((n,))] * 4
        + [dma((ny, n))] * 4
        + [dma((ny, nz))] * 4
        + [dma((n,))] * 2
        + [dma((ny,))] * 4
        + [dma((n,))] * 6,
        compiler_params=pltpu.CompilerParams(
            collective_id=0, has_side_effects=True, vmem_limit_bytes=LIMIT
        ),
    )(ids, weights, decay, rows, grad, kept, gate_w, up_w, down_w)


def tail_kernel(
    n, ny, stream_ref, state_ref, cols_ref, states_ref,
    local_sem, a_send, a_recv, i_send, i_recv, p_send, p_recv,
):
    s, t, y, c = where_am_i(n, ny)
    half = stream_ref.shape[1] // 2
    partner = (s, y * 2 + 1 - c)
    greet(sp_peers(n, s, t) + [partner])
    band = pl.ds(pl.multiple_of(c * half, half), half)
    own = [
        pltpu.make_async_copy(stream_ref.at[s], cols_ref.at[s], local_sem.at[0]),
        pltpu.make_async_copy(state_ref, states_ref.at[s], local_sem.at[1]),
    ]
    for copy in own:
        copy.start()
    waits, arrivals = [copy.wait for copy in own], []
    for k in range(1, n):
        peer = lax.rem(s + k, n)
        copy = remote(state_ref, states_ref.at[s], i_send.at[k], i_recv.at[k], (peer, t))
        copy.start()
        waits.append(copy.wait)
    for k in range(1, n):
        peer = lax.rem(s + k, n)
        copy = remote(
            stream_ref.at[peer, band], cols_ref.at[s, band], a_send.at[k], a_recv.at[k], (peer, t)
        )
        copy.start()
        waits.append(copy.wait_send)
        arrivals.append(copy)
    for k in range(1, n):
        arrivals[k - 1].wait_recv()
        held = cols_ref.at[lax.rem(s - k + n, n), band]
        copy = remote(held, held, p_send.at[k], p_recv.at[k], partner)
        copy.start()
        waits.append(copy.wait)
    for wait in waits:
        wait()


def tail_exchange(n, ny, stream, state):
    dma = pltpu.SemaphoreType.DMA
    return pl.pallas_call(
        functools.partial(tail_kernel, n, ny),
        out_shape=(
            jax.ShapeDtypeStruct(stream.shape, BF16),
            jax.ShapeDtypeStruct((n,) + state.shape, state.dtype),
        ),
        in_specs=[pl.BlockSpec(memory_space=pltpu.VMEM)] * 2,
        out_specs=[pl.BlockSpec(memory_space=pltpu.VMEM)] * 2,
        scratch_shapes=[dma((2,))] + [dma((n,))] * 6,
        compiler_params=pltpu.CompilerParams(
            collective_id=2, has_side_effects=True, vmem_limit_bytes=LIMIT
        ),
    )(stream, state)


def on_device(
    moe_input,
    out_grad,
    expert_ids,
    expert_weights,
    w_gate,
    w_up,
    w_down,
    out_proj,
    retained,
    queries,
    keys,
    values,
    log_decay,
    incoming_state,
):
    f32 = jnp.float32
    bf16 = jnp.bfloat16
    upper_limit = lax.Precision.HIGHEST
    tokens_here = moe_input.shape[0]
    sp_count = lax.axis_size("sp")
    tp_count = lax.axis_size("tp")
    capacity = -(-(5 * tokens_here // (2 * sp_count)) // 16) * 16
    along = (((0,), (0,)), ((), ()))
    ny = tp_count // 2
    heads_here = log_decay.shape[1]
    running_total = jnp.cumsum(log_decay, axis=0)
    last_sum = running_total[-1]
    stream, stream_blocks, kept_all, ends_all, gate_w_grad, up_w_grad, down_grad = main_part(
        sp_count, ny, capacity, expert_ids.T, expert_weights.T, log_decay.T, moe_input, out_grad,
        retained, w_gate, w_up, w_down,
    )
    ret_grad = lax.dot_general(
        stream, out_proj, (((1,), (1,)), ((), ())), preferred_element_type=f32
    ).astype(bf16)
    key_dim = queries.shape[1] // heads_here
    value_dim = values.shape[1] // heads_here
    query_rows = queries.astype(f32).reshape(tokens_here, heads_here, key_dim)
    key_matrix = keys.astype(f32).reshape(tokens_here, heads_here, key_dim)
    value_matrix = values.astype(f32).reshape(tokens_here, heads_here, value_dim)
    incoming_gradient = ret_grad.astype(f32).reshape(tokens_here, heads_here, value_dim)
    place = jnp.arange(tokens_here)
    causal = (place[:, None] >= place[None, :])[:, :, None]
    diff = running_total[:, None, :] - running_total[None, :, :]
    decay = jnp.where(causal, jnp.exp(jnp.minimum(diff, 0.0)), 0.0)
    scores = jnp.einsum("thk,shk->tsh", query_rows, key_matrix, precision=upper_limit) * decay
    prob_grad = (
        jnp.einsum("thv,shv->tsh", incoming_gradient, value_matrix, precision=upper_limit) * decay
    )
    added_input = jnp.einsum(
        "yb,ybm,ybx->bmx",
        jnp.exp(running_total),
        query_rows,
        incoming_gradient,
        precision=upper_limit,
    )
    flat_state = added_input.transpose(1, 0, 2).reshape(key_dim, heads_here * value_dim)
    stream_all, states = tail_exchange(sp_count, ny, stream_blocks, flat_state.astype(bf16))
    out_proj_grad = lax.dot_general(
        stream_all.reshape(sp_count * tokens_here, -1),
        kept_all.reshape(sp_count * tokens_here, -1),
        along,
        preferred_element_type=f32,
    )
    block_ends = ends_all[:, :heads_here, 0]
    before = jnp.cumsum(block_ends, axis=0) - block_ends
    here = lax.axis_index("sp")
    since = jnp.sum(
        jnp.where(jnp.arange(sp_count)[:, None] <= here, block_ends, 0.0), axis=0, keepdims=True
    )
    reach = jnp.where(
        jnp.arange(sp_count)[:, None] > here, jnp.exp(jnp.minimum(before - since, 0.0)), 0.0
    )
    state_gradient = jnp.sum(
        states.astype(f32).reshape(sp_count, key_dim, heads_here, value_dim)
        * reach[:, None, :, None],
        axis=0,
    ).transpose(1, 0, 2)
    tail = jnp.exp(last_sum[None, :] - running_total)[..., None]
    query_grad = jnp.einsum("tsh,shk->thk", prob_grad, key_matrix, precision=upper_limit) + jnp.exp(
        running_total
    )[..., None] * jnp.einsum(
        "ybc,bfc->ybf", incoming_gradient, incoming_state[0], precision=upper_limit
    )
    key_grad = jnp.einsum(
        "tsh,thk->shk", prob_grad, query_rows, precision=upper_limit
    ) + tail * jnp.einsum("rgd,gnd->rgn", value_matrix, state_gradient, precision=upper_limit)
    value_grad = jnp.einsum(
        "tsh,thv->shv", scores, incoming_gradient, precision=upper_limit
    ) + tail * jnp.einsum("bgi,gie->bge", key_matrix, state_gradient, precision=upper_limit)
    return (
        gate_w_grad,
        up_w_grad,
        down_grad,
        out_proj_grad,
        query_grad.reshape(tokens_here, -1).astype(bf16),
        key_grad.reshape(tokens_here, -1).astype(bf16),
        value_grad.reshape(tokens_here, -1).astype(bf16),
    )


def solution(mesh):
    placed = (
        P("sp", None),
        P("sp", "tp"),
        P("sp", None),
        P("sp", None),
        P("sp", None, "tp"),
        P("sp", None, "tp"),
        P("sp", "tp", None),
        P("tp", None),
        P("sp", "tp"),
        P("sp", "tp"),
        P("sp", "tp"),
        P("sp", "tp"),
        P("sp", "tp"),
        P("sp", "tp", None, None),
    )
    return jax.shard_map(
        on_device,
        mesh=mesh,
        in_specs=placed,
        out_specs=(
            P("sp", None, "tp"),
            P("sp", None, "tp"),
            P("sp", "tp", None),
            P("sp", "tp"),
            P("sp", "tp"),
            P("sp", "tp"),
            P("sp", "tp"),
        ),
        check_vma=False,
    )
```

time: 151 us -> 127 us (0.84)
  matrix products: 28.5 us -> 10.6 us
  Pallas kernels: 108 us -> 99.3 us
  local copies, waits for them, and re-layouts: 8.04 us -> 12.9 us
  other arithmetic: 4.81 us -> 2.84 us
    dot_general x8 -> x0, matrix products: 19.4 us -> none  [the longest x1 4.35 us: expert_back(): lax.dot_general(rows, up_grad, along, preferred_element_type=f32)]
    pallas_call x2 -> x1, Pallas kernels: 86.6 us -> 77.4 us  [main_part(): pl.pallas_call(functools.partial(main_kernel, n, ny, cap), out_shape=(jax...]
    unnamed x43 -> x31, local copies, waits for them, and re-layouts: 5.33 us -> 10.1 us
where the time goes in v1:
time: 127 us
  Pallas kernels  99.3 us (78%)
  local copies, waits for them, and re-layouts  12.9 us (10%)
  matrix products  10.6 us (8%)
  other arithmetic  2.84 us (2%)
    pallas_call x1, Pallas kernels, main_part(): pl.pallas_call(functools.partial(main_kernel, n, ny, cap), out_shape=(jax...  77.4 us
    pallas_call x1, Pallas kernels, tail_exchange(): pl.pallas_call(functools.partial(tail_kernel, n, ny), out_shape=(jax.Shap...  21.9 us
    unnamed x31, local copies, waits for them, and re-layouts  10.1 us
    dot_general x1, matrix products, on_device(): lax.dot_general(stream_all.reshape(sp_count * tokens_here, -1), kept_all....  2.77 us

profile of v1, /device:TPU:0, one launch (start us, length us, event | category | flops | bytes accessed | tf_op | source)
XLA Modules:
  0.0 126.5 jit_solution(9934333699488068590)
XLA Ops:
  0.6 0.0 copy-start
  0.6 0.8 pad.3
  1.5 1.2 reduce-window.6
  2.7 0.1 slice.21
  2.8 0.1 copy.87
  2.9 0.1 copy.88
  3.0 0.1 add_bitcast_fusion
  3.1 0.2 slice_reduce_fusion
  3.3 0.1 subtract_exponential_fusion
  3.3 77.4 %shard_map.189 = (bf16[192,2048]{1,0:T(8,128)(2,1)}, bf16[8,192,256]{2,1,0:T(8,128)(2,1)}, bf16[8,192,384]{2,1,0:T(8,128)(2,1)}, f32[8,8,128]{2,1,0:T(8,128)}, b...) custom-call(s32[2,192]{1,0:T(2,128)} %bitcast.104, f32[2,192]{1,0:T(2,128)} %bitcast.105, ...), custom_call_target="tpu_custom_call" | custom-call | tf_op jit(solution)/shard_map/pallas_call | solution.py:400
  80.8 0.0 copy-start.8
  80.8 1.8 %convolution_convert_fusion = bf16[192,384]{1,0:T(8,128)(2,1)S(1)} fusion(bf16[192,2048]{1,0:T(8,128)(2,1)} %get-tuple-element.20, bf16[384,2048]{1,0:T(8,128)(2,1)S(1)} %copy-done), kind=kOutput, calls=%fused_computation.10 | convolution fusion | flops 302063616 | bytes 2506752 | tf_op jit(solution)/shard_map/dot_general | solution.py:531
  82.7 0.1 copy.107
  82.8 0.1 copy.89
  82.9 0.3 fusion.11
  83.3 0.7 convert_element_type.38.state_ref
  84.0 21.9 %shard_map.190 = (bf16[8,192,256]{2,1,0:T(8,128)(2,1)}, bf16[8,48,384]{2,1,0:T(8,128)(2,1)}) custom-call(bf16[8,192,256]{2,1,0:T(8,128)(2,1)} %get-tuple-element.19.stream_ref, bf16[48,384]{1,0:T(8,128)(2,1)} %convert_element_type.38.state_ref), custom_call_target="tpu_custom_call" | custom-call | tf_op jit(solution)/shard_map/pallas_call | solution.py:484
  105.9 0.1 copy.96
  106.0 0.1 select_reduce_fusion
  106.1 0.2 reduce_window_sum.31
  106.3 0.1 exponential_select_fusion.1
  106.4 0.1 copy.97
  106.4 0.1 mul.44
  106.5 0.1 mul.45
  106.6 1.0 multiply_reduce_fusion
  107.7 0.1 reduce_sum.22
  107.8 0.1 copy.94
  107.9 0.0 copy-start.9
  107.9 0.4 fusion
  108.3 0.4 convolution_bitcast_fusion.4
  108.7 0.4 fusion.4
  109.1 0.8 copy.105
  109.9 0.1 reshape.120
  110.1 0.0 copy-start.5
  110.1 0.7 copy-done.5
  110.8 0.5 fusion.7
  111.2 1.4 %fusion.1 = f32[192,192,4]{1,0,2:T(8,128)S(1)} fusion(bf16[192,4,96]{0,2,1:T(8,128)(2,1)S(1)} %bitcast.85, f32[192,4]{0,1:T(4,128)S(1)} %get-tuple-element.55, pred[192,192]{1,0:T(8,128)(4,1)} %copy-done.9, bf16[192,4,96]{2,1,0:T(4,128)(2,1)} %copy-done.5), kind=kOutput, calls=%fused_computation.3 | convolution fusion | flops 28901376 | bytes 924672 | tf_op jit(solution)/shard_map/thv,shv->tsh/dot_general | solution.py:546
  112.6 1.1 fusion.10
  113.7 1.6 %copy.104 = bf16[192,192]{1,0:T(8,128)(2,1)} copy(bf16[192,192]{0,1:T(8,128)(2,1)} %bitcast.97) | data formatting | bytes 147456
  115.3 1.1 fusion.8
  116.4 0.5 fusion.9
  117.0 0.7 copy.103
  117.7 2.8 %convolution_bitcast_fusion.2 = f32[256,384]{1,0:T(8,128)} fusion(bf16[8,192,256]{2,1,0:T(8,128)(2,1)S(1)} %copy-done.4, bf16[8,192,384]{2,1,0:T(8,128)(2,1)} %get-tuple-element.22), kind=kOutput, calls=%fused_computation.4 | convolution fusion | flops 301989888 | bytes 2359296 | tf_op jit(solution)/shard_map/dot_general | solution.py:557
  120.5 1.3 %copy.122 = bf16[1,2048,512]{2,1,0:T(8,128)(2,1)} copy(bf16[1,2048,512]{2,1,0:T(8,128)(2,1)S(1)} %copy-done.3) | data formatting | bytes 4194304
  121.8 1.0 copy-done.2
  122.9 1.3 %copy.123 = bf16[1,2048,512]{2,1,0:T(8,128)(2,1)} copy(bf16[1,2048,512]{2,1,0:T(8,128)(2,1)S(1)} %copy-done.2) | data formatting | bytes 4194304
  124.2 1.0 copy-done.1
  125.2 1.3 %copy.124 = bf16[1,512,2048]{2,1,0:T(8,128)(2,1)} copy(bf16[1,512,2048]{2,1,0:T(8,128)(2,1)S(1)} %copy-done.1) | data formatting | bytes 4194304
  (23 shorter events, 0.2 us)
Async XLA Ops:
  0.6 80.2 %copy-start = (bf16[384,2048]{1,0:T(8,128)(2,1)S(1)}, bf16[384,2048]{1,0:T(8,128)(2,1)}, u32[]{:S(2)}) copy-start(bf16[384,2048]{1,0:T(8,128)(2,1)} %param.21) | copy-start | bytes 4718596
  80.8 2.0 %copy-start.7 = (bf16[192,192]{1,0:T(8,128)(2,1)S(1)}, bf16[192,192]{1,0:T(8,128)(2,1)}, u32[]{:S(2)}) copy-start(bf16[192,192]{1,0:T(8,128)(2,1)} %param.23) | copy-start | bytes 221188
  80.8 25.1 %copy-start.10 = (f32[8,8,128]{2,1,0:T(8,128)S(1)}, f32[8,8,128]{2,1,0:T(8,128)}, u32[]{:S(2)}) copy-start(f32[8,8,128]{2,1,0:T(8,128)} %get-tuple-element.24) | copy-start | bytes 98308
  80.8 27.0 %copy-start.8 = (bf16[192,192]{1,0:T(8,128)(2,1)S(1)}, bf16[192,192]{1,0:T(8,128)(2,1)}, u32[]{:S(2)}) copy-start(bf16[192,192]{1,0:T(8,128)(2,1)} %param.24) | copy-start | bytes 221188
  107.8 2.1 %copy-start.6 = (bf16[192,384]{1,0:T(8,128)(2,1)S(1)}, bf16[192,384]{1,0:T(8,128)(2,1)}, u32[]{:S(2)}) copy-start(bf16[192,384]{1,0:T(8,128)(2,1)} %param.25) | copy-start | bytes 442372
  107.9 0.8 copy-start.9
  110.1 0.7 copy-start.5
  111.2 6.5 %copy-start.4 = (bf16[8,192,256]{2,1,0:T(8,128)(2,1)S(1)}, bf16[8,192,256]{2,1,0:T(8,128)(2,1)}, u32[]{:S(2)}) copy-start(bf16[8,192,256]{2,1,0:T(8,128)(2,1)} %get-tuple-element.21) | copy-start | bytes 2359300
  117.7 2.8 %copy-start.3 = (bf16[1,2048,512]{2,1,0:T(8,128)(2,1)S(1)}, bf16[1,2048,512]{2,1,0:T(8,128)(2,1)}, u32[]{:S(2)}) copy-start(bf16[1,2048,512]{2,1,0:T(8,128)(2,1)} %get-tuple-element.65) | copy-start | bytes 6291460
  120.5 2.3 %copy-start.2 = (bf16[1,2048,512]{2,1,0:T(8,128)(2,1)S(1)}, bf16[1,2048,512]{2,1,0:T(8,128)(2,1)}, u32[]{:S(2)}) copy-start(bf16[1,2048,512]{2,1,0:T(8,128)(2,1)} %get-tuple-element.66) | copy-start | bytes 6291460
  122.9 2.3 %copy-start.1 = (bf16[1,512,2048]{2,1,0:T(8,128)(2,1)S(1)}, bf16[1,512,2048]{2,1,0:T(8,128)(2,1)}, u32[]{:S(2)}) copy-start(bf16[1,512,2048]{2,1,0:T(8,128)(2,1)} %get-tuple-element.67) | copy-start | bytes 6291460

commit v2 on v1

--- a/solution.py
+++ b/solution.py
@@ -10,7 +10,7 @@
 MESH = pl.DeviceIdType.MESH
 F32 = jnp.float32
 BF16 = jnp.bfloat16
-LIMIT = 60 * 1024 * 1024
+LIMIT = 38 * 1024 * 1024
 
 
 def where_am_i(n, ny):
@@ -57,18 +57,21 @@
 
 
 def main_kernel(
-    n, ny, cap, ids_ref, weights_ref, decay_ref, rows_hbm, grad_ref, kept_ref,
-    gate_hbm, up_hbm, down_hbm,
-    stream_ref, blocks_ref, kept_out, ends_out, gate_grad_ref, up_grad_ref, down_grad_ref,
-    rows_v, gate_w, up_w, down_w, pick, send, slots, act, both_grads, part, near, pairs, far,
+    n, ny, cap, ids_hbm, weights_hbm, decay_hbm, rows_hbm, grad_hbm, kept_hbm,
+    gate_hbm, up_hbm, down_hbm, proj_hbm, query_hbm, key_hbm, value_hbm, incoming_hbm,
+    kept_out, cols_ref, gate_grad_ref, up_grad_ref, down_grad_ref, query_out, key_out, value_out,
+    stream_ref, ends_out, proj, incoming, o_ref, states, pair_state, reach, turn_out, turn_in,
+    blocks, ids_ref, weights_ref, decay_ref, grad_ref, kept_ref, query_ref, key_ref, value_ref,
+    incoming_ref, rows_v, gate_w, up_w, down_w, pick, send, slots, act, both_grads, part, near, pairs, far,
     share, back,
     load_sem, a_send, a_recv, e_send, e_recv, y_send, y_recv, p_send, p_recv,
     n_send, n_recv, f_send, f_recv, b_send, b_recv, g_send, g_recv, h_send, h_recv,
     r_send, r_recv, l_send, l_recv, x_send, x_recv,
+    s_send, s_recv, u_send, u_recv, c_send, c_recv, v_send, v_recv, w_send, w_recv,
 ):
     s, t, y, c = where_am_i(n, ny)
-    q = grad_ref.shape[1]
-    heads, tokens = decay_ref.shape
+    tokens, q = grad_ref.shape
+    heads = decay_ref.shape[0]
     width = gate_w.shape[1]
     nz = n // 2
     z, x = lax.div(s, 2), lax.rem(s, 2)
@@ -101,16 +104,22 @@
     for peer in peers:
         pl.semaphore_signal(barrier, inc=1, device_id=peer, device_id_type=MESH)
 
-    own_rows = pltpu.make_async_copy(rows_hbm.at[:, columns(t)], rows_v, load_sem.at[0])
-    own_rows.start()
     loads = [
-        pltpu.make_async_copy(hbm, local, load_sem.at[1 + j])
+        pltpu.make_async_copy(hbm, local, load_sem.at[j])
         for j, (hbm, local) in enumerate(
-            [(gate_hbm.at[0], gate_w), (up_hbm.at[0], up_w), (down_hbm.at[0], down_w)]
+            [
+                (ids_hbm, ids_ref), (weights_hbm, weights_ref), (decay_hbm, decay_ref),
+                (grad_hbm, grad_ref), (rows_hbm.at[:, columns(t)], rows_v), (kept_hbm, kept_ref),
+                (gate_hbm.at[0], gate_w), (up_hbm.at[0], up_w), (down_hbm.at[0], down_w),
+                (proj_hbm, proj), (query_hbm, query_ref), (key_hbm, key_ref),
+                (value_hbm, value_ref), (incoming_hbm, incoming_ref),
+            ]
         )
     ]
     for copy in loads:
         copy.start()
+    for copy in loads[:6]:
+        copy.wait()
 
     ids = ids_ref[...].astype(F32)
     ids = [ids[j : j + 1, :] for j in range(2)]
@@ -138,7 +147,6 @@
     )
     cotangent = jnp.dot(picker, grad_ref[...], preferred_element_type=F32) * slot_weight
     send[:, 1] = cotangent.astype(BF16).reshape(n, cap, q)
-    own_rows.wait()
     picked = jnp.dot(picker, rows_v[...], preferred_element_type=F32).astype(BF16)
     send[:, 0] = picked.reshape(n, cap, q)
     slots[0, block_rows(s), columns(t)] = send[s, 0]
@@ -342,16 +350,22 @@
         count = gate_grad_ref.shape[1] // tall
         lax.fori_loop(lo * count // 4, hi * count // 4, step, 0)
 
+    ends_moving = []
     for k in range(1, n):
         to = lax.rem(s + k, n)
-        go(remote(ends_out.at[s], ends_out.at[s], e_send.at[k], e_recv.at[k], (to, t)), "wait")
+        ends_moving.append(
+            go(
+                remote(ends_out.at[s], ends_out.at[s], e_send.at[k], e_recv.at[k], (to, t)),
+                "wait_send",
+            )
+        )
     kept_start()
     for i in range(nz + 1):
         if i < nz:
             arrive(i, 0)
             arrive(i, 1)
         if i == 1:
-            for copy in loads:
+            for copy in loads[6:]:
                 copy.wait()
         if i >= 1:
             relay(i - 1, 0)
@@ -378,39 +392,273 @@
     outer = {}
     for d in range(1, ny):
         outer[d] = go(remote(mine, mine, g_send.at[d], g_recv.at[d], away(d)), "wait_send")
-    go(remote(mine, mine, h_send.at[0], h_recv.at[0], partner), "wait")
+    inner = {}
+    inner[0] = go(remote(mine, mine, h_send.at[0], h_recv.at[0], partner), "wait_send")
     in_grads(2, 4)
     for d in range(1, ny):
         outer[d].wait_recv()
         theirs = stream_ref.at[:, columns(lax.rem(y - d + ny, ny) * 2 + c)]
-        go(remote(theirs, theirs, h_send.at[d], h_recv.at[d], partner), "wait")
+        inner[d] = go(
+            remote(theirs, theirs, h_send.at[d], h_recv.at[d], partner), "wait_send"
+        )
+    band_count = 2 * ny if tokens % (32 * ny) == 0 else 2
+    tall = tokens // band_count
+    wide = cols_ref.shape[2]
+    tp_bands = band_count > 2
+
+    def band(yy, cc):
+        return pl.ds(pl.multiple_of((yy * 2 + cc if tp_bands else cc) * tall, tall), tall)
+
+    value_dim, key_dim = value_ref.shape[1] // heads, key_ref.shape[1] // heads
+    ret = lax.dot_general(
+        stream_ref[:, columns(t)], proj[:, columns(t)], across_dims, preferred_element_type=F32
+    )
+    for d in range(1, ny):
+        tt = lax.rem(y - d + ny, ny) * 2 + c
+        ret = ret + lax.dot_general(
+            stream_ref[:, columns(tt)], proj[:, columns(tt)], across_dims,
+            preferred_element_type=F32,
+        )
+    for d in range(ny):
+        inner[d].wait_recv()
+        tt = lax.rem(y - d + ny, ny) * 2 + 1 - c
+        ret = ret + lax.dot_general(
+            stream_ref[:, columns(tt)], proj[:, columns(tt)], across_dims,
+            preferred_element_type=F32,
+        )
+    o_ref[...] = ret.astype(BF16)
+
+    def expand(rows, width, depth):
+        lane = lax.div(lax.broadcasted_iota(jnp.int32, (rows[0].shape[0], width), 1), depth)
+        out = jnp.zeros((rows[0].shape[0], width), F32)
+        for h in range(heads):
+            out = jnp.where(lane == h, jnp.broadcast_to(rows[h], out.shape), out)
+        return out
+
+    key_width, value_width = heads * key_dim, heads * value_dim
+    exact = lax.Precision.HIGHEST
+    low = (first >= second).astype(F32)
+    total = lax.dot_general(
+        low, decay_ref[...], across_dims, precision=exact, preferred_element_type=F32
+    )
+    total_row = lax.dot_general(
+        decay_ref[...], low, across_dims, precision=exact, preferred_element_type=F32
+    )
+    head_total = [total[:, h : h + 1] for h in range(heads)]
+    head_row = [total_row[h : h + 1, :] for h in range(heads)]
+    head_end = [total[tokens - 1 : tokens, h : h + 1] for h in range(heads)]
+    grown = jnp.exp(expand(head_total, key_width, key_dim))
+    state_row = lax.div(lax.broadcasted_iota(jnp.int32, (key_width, value_width), 0), key_dim)
+    state_lane = lax.div(lax.broadcasted_iota(jnp.int32, (key_width, value_width), 1), value_dim)
+    diagonal = state_row == state_lane
+    injected = lax.dot_general(
+        (query_ref[...].astype(F32) * grown).astype(BF16), o_ref[...], along_dims,
+        preferred_element_type=F32,
+    )
+    injected = jnp.where(diagonal, injected, 0.0)
+    folded = injected[:key_dim, :]
+    for h in range(1, heads):
+        folded = folded + injected[h * key_dim : (h + 1) * key_dim, :]
+    states[z] = folded.astype(BF16)
+    pair_copy = go(
+        remote(states.at[z], pair_state, u_send.at[0], u_recv.at[0], (z * 2 + 1 - x, t)),
+        "wait_send",
+    )
+    for i in range(1, nz):
+        go(
+            remote(
+                states.at[z], states.at[z], s_send.at[i], s_recv.at[z], (order[i] * 2 + x, t)
+            ),
+            "wait_send",
+        )
+
+    def piece(b, rows):
+        if wide % 128:
+            return blocks.at[b, rows]
+        return stream_ref.at[rows, pl.ds(pl.multiple_of(b * wide, wide), wide)]
+
+    if wide % 128:
+        for b in range(n):
+            blocks[b] = stream_ref[:, b * wide : (b + 1) * wide]
+
+    for i in range(nz):
+        for e in range(2):
+            if (i, e) != (0, 0):
+                to = member(i, e)
+                go(
+                    remote(
+                        piece(to, band(y, c)), cols_ref.at[s, band(y, c)],
+                        c_send.at[2 * i + e], c_recv.at[s], (to, t),
+                    ),
+                    "wait_send",
+                )
+    cols_ref[s] = piece(s, pl.ds(0, tokens))[...]
+
+    for copy in ends_moving:
+        copy.wait_recv()
+    before = [jnp.zeros((1, value_width), F32)]
+    since = jnp.zeros((1, value_width), F32)
+    for b in range(n):
+        ends = expand([ends_out[b, h : h + 1, 0:1] for h in range(heads)], value_width, value_dim)
+        before.append(before[-1] + ends)
+        since = since + ends * below(b, 2 * z + 2, 2 * n).astype(F32)
+    for b in range(n):
+        reach[b] = jnp.broadcast_to(
+            jnp.exp(jnp.minimum(before[b] - since, 0.0)) * below(2 * z + 1, b, 2 * n).astype(F32),
+            (8, value_width),
+        )
+
+    key_lane = lax.div(lax.broadcasted_iota(jnp.int32, (tokens, key_width), 1), key_dim)
+    value_lane = lax.div(lax.broadcasted_iota(jnp.int32, (tokens, value_width), 1), value_dim)
+
+    def only(values, lane, h):
+        return jnp.where(lane == h, values, jnp.zeros_like(values))
+
+    place = lax.broadcasted_iota(jnp.int32, (value_dim, value_width), 0)
+    spot = lax.broadcasted_iota(jnp.int32, (value_dim, value_width), 1)
+    for h in range(heads):
+        put = (place + h * value_dim == spot).astype(F32).astype(BF16)
+        incoming[h * key_dim : (h + 1) * key_dim, :] = jnp.dot(
+            incoming_ref[0, h].astype(BF16), put, preferred_element_type=F32
+        ).astype(BF16)
+    query_grad = grown * lax.dot_general(
+        o_ref[...], incoming[...], across_dims, preferred_element_type=F32
+    )
+    key_grad = jnp.zeros((tokens, key_width), F32)
+    value_grad = jnp.zeros((tokens, value_width), F32)
+    for h in range(heads):
+        o_head = only(o_ref[...], value_lane, h)
+        v_head = only(value_ref[...], value_lane, h)
+        q_head = only(query_ref[...], key_lane, h)
+        k_head = only(key_ref[...], key_lane, h)
+        diff = head_total[h] - head_row[h]
+        fade = jnp.where(first >= second, jnp.exp(jnp.minimum(diff, 0.0)), 0.0)
+        fade_turned = jnp.where(first <= second, jnp.exp(jnp.minimum(-diff, 0.0)), 0.0)
+        prob = lax.dot_general(o_head, value_ref[...], across_dims, preferred_element_type=F32)
+        query_grad = query_grad + jnp.dot(
+            (prob * fade).astype(BF16), k_head, preferred_element_type=F32
+        )
+        prob = lax.dot_general(v_head, o_ref[...], across_dims, preferred_element_type=F32)
+        key_grad = key_grad + jnp.dot(
+            (prob * fade_turned).astype(BF16), q_head, preferred_element_type=F32
+        )
+        score = lax.dot_general(k_head, query_ref[...], across_dims, preferred_element_type=F32)
+        value_grad = value_grad + jnp.dot(
+            (score * fade_turned).astype(BF16), o_head, preferred_element_type=F32
+        )
+    query_out[...] = query_grad.astype(BF16)
+
+    later = jnp.zeros((key_dim, value_width), F32)
+    for i in range(1, nz):
+        src = order[i]
+        remote(
+            states.at[src], states.at[src], s_send.at[i], s_recv.at[src], (src * 2 + x, t)
+        ).wait_recv()
+        later = later + reach[src * 2 + x][0:1, :] * states[src].astype(F32)
+    turn_out[...] = later.astype(BF16)
+    turned = go(
+        remote(turn_out, turn_in, u_send.at[1], u_recv.at[1], (z * 2 + 1 - x, t)), "wait_send"
+    )
+
+    from_far, from_partner = {}, {}
+    for i in range(nz):
+        for e in range(2):
+            if (i, e) == (0, 0):
+                continue
+            src, k = member(i, e), 2 * i + e
+            mine = cols_ref.at[src, band(y, c)]
+            remote(
+                piece(src, band(y, c)), mine, c_send.at[k], c_recv.at[src],
+                (src, t),
+            ).wait_recv()
+            if tp_bands:
+                for d in range(1, ny):
+                    from_far[d, k] = go(
+                        remote(mine, mine, v_send.at[d, k], v_recv.at[d, k], away(d)),
+                        "wait_send",
+                    )
+            go(remote(mine, mine, w_send.at[0, k], w_recv.at[0, k], partner), "wait")
+    turned.wait_recv()
+    later = turn_out[...].astype(F32) + turn_in[...].astype(F32)
+    lower = (1 - x).astype(F32)
+    pair_ends = expand(
+        [ends_out[z * 2 + 1, h : h + 1, 0:1] for h in range(heads)], value_width, value_dim
+    )
+    pair_copy.wait_recv()
+    later = jnp.exp(lower * pair_ends) * later + lower * pair_state[...].astype(F32)
+    stacked = jnp.concatenate([later.astype(BF16)] * heads, axis=0)
+    stacked = jnp.where(diagonal, stacked, jnp.zeros_like(stacked))
+    left = [end - own for end, own in zip(head_end, head_total)]
+    key_grad = key_grad + jnp.exp(expand(left, key_width, key_dim)) * lax.dot_general(
+        value_ref[...], stacked, across_dims, preferred_element_type=F32
+    )
+    key_out[...] = key_grad.astype(BF16)
+    value_grad = value_grad + jnp.exp(expand(left, value_width, value_dim)) * jnp.dot(
+        key_ref[...], stacked, preferred_element_type=F32
+    )
+    value_out[...] = value_grad.astype(BF16)
+    if tp_bands:
+        for i in range(nz):
+            for e in range(2):
+                if (i, e) == (0, 0):
+                    continue
+                src, k = member(i, e), 2 * i + e
+                for d in range(1, ny):
+                    from_far[d, k].wait_recv()
+                    theirs = cols_ref.at[src, band(lax.rem(y - d + ny, ny), c)]
+                    go(
+                        remote(theirs, theirs, w_send.at[d, k], w_recv.at[d, k], partner), "wait"
+                    )
     for wait in waits:
         wait()
-    wide = blocks_ref.shape[2]
-    for b in range(n):
-        blocks_ref[b] = stream_ref[:, b * wide : (b + 1) * wide]
-
-
-def main_part(n, ny, cap, ids, weights, decay, rows, grad, kept, gate_w, up_w, down_w):
+
+
+def main_part(
+    n, ny, cap, ids, weights, decay, rows, grad, kept, gate_w, up_w, down_w, proj, query, key,
+    value, incoming,
+):
     tokens, q = grad.shape
+    heads = decay.shape[0]
     dma = pltpu.SemaphoreType.DMA
     slots, model, width = n * cap, rows.shape[1], gate_w.shape[2]
     nz = n // 2
-    vmem, anywhere = pl.BlockSpec(memory_space=pltpu.VMEM), pl.BlockSpec(memory_space=pl.ANY)
+    state = (key.shape[1] // heads, value.shape[1])
+    vmem = pl.BlockSpec(memory_space=pltpu.VMEM)
     return pl.pallas_call(
         functools.partial(main_kernel, n, ny, cap),
         out_shape=(
-            jax.ShapeDtypeStruct((tokens, model), BF16),
+            jax.ShapeDtypeStruct((n,) + kept.shape, BF16),
             jax.ShapeDtypeStruct((n, tokens, model // n), BF16),
-            jax.ShapeDtypeStruct((n,) + kept.shape, BF16),
-            jax.ShapeDtypeStruct((n, 8, 128), F32),
             jax.ShapeDtypeStruct(gate_w.shape, BF16),
             jax.ShapeDtypeStruct(up_w.shape, BF16),
             jax.ShapeDtypeStruct(down_w.shape, BF16),
+            jax.ShapeDtypeStruct(query.shape, BF16),
+            jax.ShapeDtypeStruct(key.shape, BF16),
+            jax.ShapeDtypeStruct(value.shape, BF16),
         ),
-        in_specs=[vmem, vmem, vmem, anywhere, vmem, vmem, anywhere, anywhere, anywhere],
-        out_specs=[vmem] * 7,
+        in_specs=[pl.BlockSpec(memory_space=pltpu.HBM)] * 14,
+        out_specs=[vmem] * 8,
         scratch_shapes=[
+            pltpu.VMEM((tokens, model), BF16),
+            pltpu.VMEM((n, 8, 128), F32),
+            pltpu.VMEM(proj.shape, BF16),
+            pltpu.VMEM((key.shape[1], value.shape[1]), BF16),
+            pltpu.VMEM((tokens, value.shape[1]), BF16),
+            pltpu.VMEM((nz,) + state, BF16),
+            pltpu.VMEM(state, BF16),
+            pltpu.VMEM((n, 8, value.shape[1]), F32),
+            pltpu.VMEM(state, BF16),
+            pltpu.VMEM(state, BF16),
+            pltpu.VMEM((n, tokens, model // n) if model // n % 128 else (1, 8, 128), BF16),
+            pltpu.VMEM(ids.shape, jnp.int32),
+            pltpu.VMEM(weights.shape, F32),
+            pltpu.VMEM(decay.shape, F32),
+            pltpu.VMEM(grad.shape, BF16),
+            pltpu.VMEM(kept.shape, BF16),
+            pltpu.VMEM(query.shape, BF16),
+            pltpu.VMEM(key.shape, BF16),
+            pltpu.VMEM(value.shape, BF16),
+            pltpu.VMEM(incoming.shape, F32),
             pltpu.VMEM((tokens, q), BF16),
             pltpu.VMEM(gate_w.shape[1:], BF16),
             pltpu.VMEM(up_w.shape[1:], BF16),
@@ -426,74 +674,63 @@
             pltpu.VMEM((ny, slots, q), BF16),
             pltpu.VMEM((slots, q), BF16),
             pltpu.VMEM((slots, q), BF16),
-            dma((4,)),
+            dma((14,)),
         ]
         + [dma((n,))] * 4
         + [dma((ny, n))] * 4
         + [dma((ny, nz))] * 4
         + [dma((n,))] * 2
         + [dma((ny,))] * 4
-        + [dma((n,))] * 6,
+        + [dma((n,))] * 6
+        + [dma((nz,))] * 2
+        + [dma((2,))] * 2
+        + [dma((n,))] * 2
+        + [dma((ny, n))] * 4,
         compiler_params=pltpu.CompilerParams(
             collective_id=0, has_side_effects=True, vmem_limit_bytes=LIMIT
         ),
-    )(ids, weights, decay, rows, grad, kept, gate_w, up_w, down_w)
-
-
-def tail_kernel(
-    n, ny, stream_ref, state_ref, cols_ref, states_ref,
-    local_sem, a_send, a_recv, i_send, i_recv, p_send, p_recv,
-):
-    s, t, y, c = where_am_i(n, ny)
-    half = stream_ref.shape[1] // 2
-    partner = (s, y * 2 + 1 - c)
-    greet(sp_peers(n, s, t) + [partner])
-    band = pl.ds(pl.multiple_of(c * half, half), half)
-    own = [
-        pltpu.make_async_copy(stream_ref.at[s], cols_ref.at[s], local_sem.at[0]),
-        pltpu.make_async_copy(state_ref, states_ref.at[s], local_sem.at[1]),
+    )(
+        *(
+            pltpu.with_memory_space_constraint(array, pltpu.HBM)
+            for array in (
+                ids, weights, decay, rows, grad, kept, gate_w, up_w, down_w, proj, query, key,
+                value, incoming,
+            )
+        )
+    )
+
+
+def final_kernel(cols_ref, kept_ref, *refs):
+    moved = len(refs) // 2
+    sources, proj_grad, targets, sems = (
+        refs[:moved - 1], refs[moved - 1], refs[moved:-1], refs[-1]
+    )
+    copies = [
+        pltpu.make_async_copy(source, target, sems.at[j])
+        for j, (source, target) in enumerate(zip(sources, targets))
     ]
-    for copy in own:
+    for copy in copies:
         copy.start()
-    waits, arrivals = [copy.wait for copy in own], []
-    for k in range(1, n):
-        peer = lax.rem(s + k, n)
-        copy = remote(state_ref, states_ref.at[s], i_send.at[k], i_recv.at[k], (peer, t))
-        copy.start()
-        waits.append(copy.wait)
-    for k in range(1, n):
-        peer = lax.rem(s + k, n)
-        copy = remote(
-            stream_ref.at[peer, band], cols_ref.at[s, band], a_send.at[k], a_recv.at[k], (peer, t)
-        )
-        copy.start()
-        waits.append(copy.wait_send)
-        arrivals.append(copy)
-    for k in range(1, n):
-        arrivals[k - 1].wait_recv()
-        held = cols_ref.at[lax.rem(s - k + n, n), band]
-        copy = remote(held, held, p_send.at[k], p_recv.at[k], partner)
-        copy.start()
-        waits.append(copy.wait)
-    for wait in waits:
-        wait()
-
-
-def tail_exchange(n, ny, stream, state):
-    dma = pltpu.SemaphoreType.DMA
+    rows = cols_ref.shape[0] * cols_ref.shape[1]
+    proj_grad[...] = lax.dot_general(
+        cols_ref[...].reshape(rows, -1), kept_ref[...].reshape(rows, -1),
+        (((0,), (0,)), ((), ())), preferred_element_type=F32,
+    )
+    for copy in copies:
+        copy.wait()
+
+
+def final_part(cols, kept, *moved):
+    vmem = pl.BlockSpec(memory_space=pltpu.VMEM)
     return pl.pallas_call(
-        functools.partial(tail_kernel, n, ny),
-        out_shape=(
-            jax.ShapeDtypeStruct(stream.shape, BF16),
-            jax.ShapeDtypeStruct((n,) + state.shape, state.dtype),
-        ),
-        in_specs=[pl.BlockSpec(memory_space=pltpu.VMEM)] * 2,
-        out_specs=[pl.BlockSpec(memory_space=pltpu.VMEM)] * 2,
-        scratch_shapes=[dma((2,))] + [dma((n,))] * 6,
-        compiler_params=pltpu.CompilerParams(
-            collective_id=2, has_side_effects=True, vmem_limit_bytes=LIMIT
-        ),
-    )(stream, state)
+        final_kernel,
+        out_shape=(jax.ShapeDtypeStruct((cols.shape[2], kept.shape[2]), F32),)
+        + tuple(jax.ShapeDtypeStruct(array.shape, array.dtype) for array in moved),
+        in_specs=[vmem] * (2 + len(moved)),
+        out_specs=[vmem] + [pl.BlockSpec(memory_space=pltpu.HBM)] * len(moved),
+        scratch_shapes=[pltpu.SemaphoreType.DMA((len(moved),))],
+        compiler_params=pltpu.CompilerParams(vmem_limit_bytes=LIMIT // 4),
+    )(cols, kept, *moved)
 
 
 def on_device(
@@ -512,89 +749,17 @@
     log_decay,
     incoming_state,
 ):
-    f32 = jnp.float32
-    bf16 = jnp.bfloat16
-    upper_limit = lax.Precision.HIGHEST
+    n, ny = lax.axis_size("sp"), lax.axis_size("tp") // 2
     tokens_here = moe_input.shape[0]
-    sp_count = lax.axis_size("sp")
-    tp_count = lax.axis_size("tp")
-    capacity = -(-(5 * tokens_here // (2 * sp_count)) // 16) * 16
-    along = (((0,), (0,)), ((), ()))
-    ny = tp_count // 2
-    heads_here = log_decay.shape[1]
-    running_total = jnp.cumsum(log_decay, axis=0)
-    last_sum = running_total[-1]
-    stream, stream_blocks, kept_all, ends_all, gate_w_grad, up_w_grad, down_grad = main_part(
-        sp_count, ny, capacity, expert_ids.T, expert_weights.T, log_decay.T, moe_input, out_grad,
-        retained, w_gate, w_up, w_down,
-    )
-    ret_grad = lax.dot_general(
-        stream, out_proj, (((1,), (1,)), ((), ())), preferred_element_type=f32
-    ).astype(bf16)
-    key_dim = queries.shape[1] // heads_here
-    value_dim = values.shape[1] // heads_here
-    query_rows = queries.astype(f32).reshape(tokens_here, heads_here, key_dim)
-    key_matrix = keys.astype(f32).reshape(tokens_here, heads_here, key_dim)
-    value_matrix = values.astype(f32).reshape(tokens_here, heads_here, value_dim)
-    incoming_gradient = ret_grad.astype(f32).reshape(tokens_here, heads_here, value_dim)
-    place = jnp.arange(tokens_here)
-    causal = (place[:, None] >= place[None, :])[:, :, None]
-    diff = running_total[:, None, :] - running_total[None, :, :]
-    decay = jnp.where(causal, jnp.exp(jnp.minimum(diff, 0.0)), 0.0)
-    scores = jnp.einsum("thk,shk->tsh", query_rows, key_matrix, precision=upper_limit) * decay
-    prob_grad = (
-        jnp.einsum("thv,shv->tsh", incoming_gradient, value_matrix, precision=upper_limit) * decay
-    )
-    added_input = jnp.einsum(
-        "yb,ybm,ybx->bmx",
-        jnp.exp(running_total),
-        query_rows,
-        incoming_gradient,
-        precision=upper_limit,
-    )
-    flat_state = added_input.transpose(1, 0, 2).reshape(key_dim, heads_here * value_dim)
-    stream_all, states = tail_exchange(sp_count, ny, stream_blocks, flat_state.astype(bf16))
-    out_proj_grad = lax.dot_general(
-        stream_all.reshape(sp_count * tokens_here, -1),
-        kept_all.reshape(sp_count * tokens_here, -1),
-        along,
-        preferred_element_type=f32,
-    )
-    block_ends = ends_all[:, :heads_here, 0]
-    before = jnp.cumsum(block_ends, axis=0) - block_ends
-    here = lax.axis_index("sp")
-    since = jnp.sum(
-        jnp.where(jnp.arange(sp_count)[:, None] <= here, block_ends, 0.0), axis=0, keepdims=True
-    )
-    reach = jnp.where(
-        jnp.arange(sp_count)[:, None] > here, jnp.exp(jnp.minimum(before - since, 0.0)), 0.0
-    )
-    state_gradient = jnp.sum(
-        states.astype(f32).reshape(sp_count, key_dim, heads_here, value_dim)
-        * reach[:, None, :, None],
-        axis=0,
-    ).transpose(1, 0, 2)
-    tail = jnp.exp(last_sum[None, :] - running_total)[..., None]
-    query_grad = jnp.einsum("tsh,shk->thk", prob_grad, key_matrix, precision=upper_limit) + jnp.exp(
-        running_total
-    )[..., None] * jnp.einsum(
-        "ybc,bfc->ybf", incoming_gradient, incoming_state[0], precision=upper_limit
-    )
-    key_grad = jnp.einsum(
-        "tsh,thk->shk", prob_grad, query_rows, precision=upper_limit
-    ) + tail * jnp.einsum("rgd,gnd->rgn", value_matrix, state_gradient, precision=upper_limit)
-    value_grad = jnp.einsum(
-        "tsh,thv->shv", scores, incoming_gradient, precision=upper_limit
-    ) + tail * jnp.einsum("bgi,gie->bge", key_matrix, state_gradient, precision=upper_limit)
-    return (
-        gate_w_grad,
-        up_w_grad,
-        down_grad,
-        out_proj_grad,
-        query_grad.reshape(tokens_here, -1).astype(bf16),
-        key_grad.reshape(tokens_here, -1).astype(bf16),
-        value_grad.reshape(tokens_here, -1).astype(bf16),
-    )
+    capacity = -(-(5 * tokens_here // (2 * n)) // 16) * 16
+    kept_all, cols, *moved = main_part(
+        n, ny, capacity, expert_ids.T, expert_weights.T, log_decay.T, moe_input, out_grad,
+        retained, w_gate, w_up, w_down, out_proj, queries, keys, values, incoming_state,
+    )
+    proj_grad, gate_grad, up_grad, down_grad, query_grad, key_grad, value_grad = final_part(
+        cols, kept_all, *moved
+    )
+    return gate_grad, up_grad, down_grad, proj_grad, query_grad, key_grad, value_grad
 
 
 def solution(mesh):

time: 127 us -> 93 us (0.73)
  local copies, waits for them, and re-layouts: 12.9 us -> 0 us
  matrix products: 10.6 us -> 0 us
  Pallas kernels: 99.3 us -> 92.1 us
  other arithmetic: 2.84 us -> 0 us
    pallas_call x1, Pallas kernels: 21.9 us -> 3.71 us  [final_part(): pl.pallas_call(final_kernel, out_shape=(jax.ShapeDtypeStruct((cols.shape[...]
    pallas_call x1, Pallas kernels: 77.4 us -> 88.4 us  [main_part(): pl.pallas_call(functools.partial(main_kernel, n, ny, cap), out_shape=(jax...]
    dot_general x11 -> x0, matrix products: 10.6 us -> none  [the longest x1 2.77 us: on_device(): lax.dot_general(stream_all.reshape(sp_count * tokens_here, -1), kept_all....]
    unnamed x31 -> x0, local copies, waits for them, and re-layouts: 10.1 us -> none
    another operation x3 -> x0, other arithmetic: 1.43 us -> none
where the time goes in v2:
time: 93 us; the launch traced here: 92.9 us
  Pallas kernels  92.1 us (99%)
    pallas_call x1, Pallas kernels, main_part(): pl.pallas_call(functools.partial(main_kernel, n, ny, cap), out_shape=(jax...  88.4 us
    pallas_call x1, Pallas kernels, final_part(): pl.pallas_call(final_kernel, out_shape=(jax.ShapeDtypeStruct((cols.shape[...  3.71 us

profile of v2, /device:TPU:0, one launch (start us, length us, event | category | flops | bytes accessed | tf_op | source)
XLA Modules:
  0.0 92.9 jit_solution(18412907661576649471)
XLA Ops:
  0.6 88.4 %shard_map.189 = (bf16[8,192,384]{2,1,0:T(8,128)(2,1)S(1)}, bf16[8,192,256]{2,1,0:T(8,128)(2,1)S(1)}, bf16[1,2048,512]{2,1,0:T(8,128)(2,1)S(1)}, bf16[1,2048,512...) custom-call(s32[2,192]{1,0:T(2,128)} %bitcast.4, ...), custom_call_target="tpu_custom_call" | custom-call | tf_op jit(solution)/shard_map/pallas_call | solution.py:627
  89.0 3.7 %shard_map.190 = (f32[256,384]{1,0:T(8,128)}, bf16[1,2048,512]{2,1,0:T(8,128)(2,1)}, bf16[1,2048,512]{2,1,0:T(8,128)(2,1)}, bf16[1,512,2048]{2,1,0:T(8,128)(2,1)...) custom-call(bf16[8,192,256]{2,1,0:T(8,128)(2,1)S(1)} %get-tuple-element.22.cols_ref, ...), custom_call_target="tpu_custom_call" | custom-call | tf_op jit(solution)/shard_map/pallas_call | solution.py:725

commit v3 on v2

--- a/solution.py
+++ b/solution.py
@@ -11,6 +11,7 @@
 F32 = jnp.float32
 BF16 = jnp.bfloat16
 LIMIT = 38 * 1024 * 1024
+AHEAD = 5
 
 
 def where_am_i(n, ny):
@@ -43,25 +44,24 @@
     return lax.div(b - a + top - 1, top)
 
 
-def nearest_first(z, nz):
-    high = nz - 1 - z
-    fewer = below(high, z, nz)
-    least = z + (high - z) * fewer
-    toward = 1 - 2 * fewer
-    order = [z]
-    for i in range(1, nz):
-        both = below(i, 2 * least + 1, 2 * nz)
-        step = (i + 1) // 2 * (1 if i % 2 else -1)
-        order.append(z + toward * (both * step + (1 - both) * (i - least)))
-    return order
+def flipped(z, i, nz):
+    if nz & (nz - 1):
+        return lax.rem(z + i, nz)
+    out, bit = 0, 1
+    while bit < nz:
+        own = lax.rem(lax.div(z, bit), 2)
+        out = out + bit * (1 - own if i & bit else own)
+        bit *= 2
+    return out
 
 
 def main_kernel(
     n, ny, cap, ids_hbm, weights_hbm, decay_hbm, rows_hbm, grad_hbm, kept_hbm,
     gate_hbm, up_hbm, down_hbm, proj_hbm, query_hbm, key_hbm, value_hbm, incoming_hbm,
-    kept_out, cols_ref, gate_grad_ref, up_grad_ref, down_grad_ref, query_out, key_out, value_out,
-    stream_ref, ends_out, proj, incoming, o_ref, states, pair_state, reach, turn_out, turn_in,
-    blocks, ids_ref, weights_ref, decay_ref, grad_ref, kept_ref, query_ref, key_ref, value_ref,
+    proj_grad, gate_grad_ref, up_grad_ref, down_grad_ref, query_out, key_out, value_out,
+    kept_out, cols_ref, stream_ref, ends_out, proj, incoming, o_ref, states, own_state, pair_state, reach, both_halves,
+    later_halves,
+    blocks, fade, fade_turned, score, ids_ref, weights_ref, decay_ref, grad_ref, kept_ref, query_ref, key_ref, value_ref,
     incoming_ref, rows_v, gate_w, up_w, down_w, pick, send, slots, act, both_grads, part, near, pairs, far,
     share, back,
     load_sem, a_send, a_recv, e_send, e_recv, y_send, y_recv, p_send, p_recv,
@@ -76,7 +76,7 @@
     nz = n // 2
     z, x = lax.div(s, 2), lax.rem(s, 2)
     partner = (s, y * 2 + 1 - c)
-    order = nearest_first(z, nz)
+    order = [flipped(z, i, nz) for i in range(nz)]
     waits = []
 
     def columns(tt):
@@ -157,14 +157,22 @@
     def block(src, tt):
         return slots.at[:, block_rows(src), columns(tt)]
 
-    for i in range(nz):
-        for e in range(2):
-            if (i, e) != (0, 0):
-                to = member(i, e)
-                go(
-                    remote(send.at[to], block(s, t), a_send.at[2 * i + e], a_recv.at[s], (to, t)),
-                    "wait_send",
-                )
+    turns = [(0, 1)]
+    for i in range(1, nz - 1, 2):
+        turns += [(i, 0), (i + 1, 0), (i, 1), (i + 1, 1)]
+    turns += [(nz - 1, 0), (nz - 1, 1)]
+    sent = []
+
+    def send_next():
+        if len(sent) < len(turns):
+            i, e = turns[len(sent)]
+            to = member(i, e)
+            copy = remote(send.at[to], block(s, t), a_send.at[2 * i + e], a_recv.at[s], (to, t))
+            copy.start()
+            sent.append(copy)
+
+    for _ in range(AHEAD):
+        send_next()
 
     def at(zz):
         return lax.rem(zz + 2 * nz, nz) * 2 + x
@@ -178,13 +186,17 @@
             "wait_send",
         )
 
+    kept_moving = []
+
     def across(held, index, source):
-        go(
-            remote(
-                source, kept_out.at[held], x_send.at[index], x_recv.at[index],
-                (z * 2 + 1 - x, t),
-            ),
-            "wait",
+        kept_moving.append(
+            go(
+                remote(
+                    source, kept_out.at[held], x_send.at[index], x_recv.at[index],
+                    (z * 2 + 1 - x, t),
+                ),
+                "wait_send",
+            )
         )
 
     right_steps, left_steps = nz // 2, nz - 1 - nz // 2
@@ -195,8 +207,6 @@
             moving["right"] = hop(0, 1, r_send, r_recv, kept_ref)
         if left_steps:
             moving["left"] = hop(0, -1, l_send, l_recv, kept_ref)
-        across(s, 0, kept_ref)
-        kept_out[s] = kept_ref[...]
 
     def kept_relay(j):
         if j <= right_steps:
@@ -229,6 +239,9 @@
         from_partner[0, k] = go(
             remote(mine, mine, p_send.at[0, k], p_recv.at[0, k], partner), "wait_send"
         )
+        if k:
+            sent[turns.index((i, e))].wait_send()
+            send_next()
 
     def relay(i, e):
         k = 2 * i + e
@@ -242,11 +255,21 @@
     across_dims = (((1,), (1,)), ((), ()))
     along_dims = (((0,), (0,)), ((), ()))
 
-    def expert(i):
-        for e in range(2):
+    units = [(i, None) for i in range(nz - 1)] + [(nz - 1, 0), (nz - 1, 1)]
+
+    def unit_rows(u):
+        i, e = units[u]
+        return chunk_rows(i) if e is None else block_rows(member(i, e))
+
+    def unit_blocks(u):
+        i, e = units[u]
+        return [(i, 0), (i, 1)] if e is None else [(i, e)]
+
+    def expert(u):
+        for i, e in unit_blocks(u):
             for d in range(ny):
                 from_partner[d, 2 * i + e].wait_recv()
-        r = chunk_rows(i)
+        r = unit_rows(u)
         gate = jnp.dot(slots[0, r, :], gate_w[...], preferred_element_type=F32)
         up = jnp.dot(slots[0, r, :], up_w[...], preferred_element_type=F32)
         act_grad = lax.dot_general(
@@ -266,42 +289,42 @@
 
     halves, summed, returns = {}, {}, {}
 
-    def swap_halves(i):
-        r = chunk_rows(i)
+    def swap_halves(u):
+        r = unit_rows(u)
         for d in list(range(1, ny)) + [0]:
             theirs = lax.rem(y + d, ny) * 2 + 1 - c
-            halves[d, i] = go(
+            halves[d, u] = go(
                 remote(
                     part.at[r, columns(theirs)], near.at[d, r, :],
-                    n_send.at[d, i], n_recv.at[d, i], partner,
+                    n_send.at[d, u], n_recv.at[d, u], partner,
                 ),
                 "wait_send",
             )
 
-    def send_pairs(i):
-        r = chunk_rows(i)
+    def send_pairs(u):
+        r = unit_rows(u)
         for d in range(1, ny):
-            halves[d, i].wait_recv()
+            halves[d, u].wait_recv()
             tt = lax.rem(y + d, ny) * 2 + c
             pairs[d, r, :] = (
                 part[r, columns(tt)].astype(F32) + near[d, r, :].astype(F32)
             ).astype(BF16)
-            summed[d, i] = go(
+            summed[d, u] = go(
                 remote(
-                    pairs.at[d, r, :], far.at[d, r, :], f_send.at[d, i], f_recv.at[d, i], (s, tt)
+                    pairs.at[d, r, :], far.at[d, r, :], f_send.at[d, u], f_recv.at[d, u], (s, tt)
                 ),
                 "wait_send",
             )
 
-    def send_back(i):
-        r = chunk_rows(i)
-        halves[0, i].wait_recv()
+    def send_back(u):
+        r = unit_rows(u)
+        halves[0, u].wait_recv()
         total = part[r, columns(t)].astype(F32) + near[0, r, :].astype(F32)
         for d in range(1, ny):
-            summed[d, i].wait_recv()
+            summed[d, u].wait_recv()
             total = total + far[d, r, :].astype(F32)
         share[r, :] = total.astype(BF16)
-        for e in range(2):
+        for i, e in unit_blocks(u):
             to = member(i, e)
             if (i, e) == (0, 0):
                 back[block_rows(s), :] = share[block_rows(s), :]
@@ -359,30 +382,64 @@
                 "wait_send",
             )
         )
+    def loaded():
+        for copy in loads[6:]:
+            copy.wait()
+
+    def forward(i):
+        relay(i, 0)
+        relay(i, 1)
+
+    def work(u):
+        expert(u)
+        swap_halves(u)
+
+    arrive(0, 0)
+    arrive(0, 1)
+    loaded()
+    kept_out[s] = kept_ref[...]
+    across(s, 0, kept_ref)
+    last = nz - 1
+    for i in range(1, last, 2):
+        arrive(i, 0)
+        arrive(i + 1, 0)
+        if i == 1:
+            forward(0)
+        arrive(i, 1)
+        if i == 1:
+            work(0)
+        else:
+            forward(i - 1)
+            send_pairs(i - 2)
+            work(i - 1)
+            send_back(i - 3)
+        arrive(i + 1, 1)
+        forward(i)
+        send_pairs(i - 1)
+        work(i)
+        if i > 1:
+            send_back(i - 2)
+    arrive(last, 0)
+    forward(last - 1)
+    send_pairs(last - 2)
+    arrive(last, 1)
     kept_start()
-    for i in range(nz + 1):
-        if i < nz:
-            arrive(i, 0)
-            arrive(i, 1)
-        if i == 1:
-            for copy in loads[6:]:
-                copy.wait()
-        if i >= 1:
-            relay(i - 1, 0)
-            relay(i - 1, 1)
-        if i >= 2:
-            send_pairs(i - 2)
-        if i >= 3:
-            send_back(i - 3)
-        if i >= 1:
-            expert(i - 1)
-            swap_halves(i - 1)
-        if i >= 2:
-            kept_relay(i - 1)
-    send_back(nz - 2) if nz > 1 else None
-    send_pairs(nz - 1)
+    work(last - 1)
+    if last > 2:
+        send_back(last - 3)
+    relay(last, 0)
+    send_pairs(last - 1)
+    work(last)
+    send_back(last - 2)
+    relay(last, 1)
+    send_pairs(last)
+    kept_relay(1)
+    work(last + 1)
+    send_back(last - 1)
+    send_pairs(last + 1)
+    send_back(last)
     down_grads()
-    send_back(nz - 1)
+    send_back(last + 1)
     in_grads(0, 2)
     token = returned(0)
     for i in range(1, nz):
@@ -395,39 +452,9 @@
     inner = {}
     inner[0] = go(remote(mine, mine, h_send.at[0], h_recv.at[0], partner), "wait_send")
     in_grads(2, 4)
-    for d in range(1, ny):
-        outer[d].wait_recv()
-        theirs = stream_ref.at[:, columns(lax.rem(y - d + ny, ny) * 2 + c)]
-        inner[d] = go(
-            remote(theirs, theirs, h_send.at[d], h_recv.at[d], partner), "wait_send"
-        )
-    band_count = 2 * ny if tokens % (32 * ny) == 0 else 2
-    tall = tokens // band_count
-    wide = cols_ref.shape[2]
-    tp_bands = band_count > 2
-
-    def band(yy, cc):
-        return pl.ds(pl.multiple_of((yy * 2 + cc if tp_bands else cc) * tall, tall), tall)
-
+    for j in range(2, nz):
+        kept_relay(j)
     value_dim, key_dim = value_ref.shape[1] // heads, key_ref.shape[1] // heads
-    ret = lax.dot_general(
-        stream_ref[:, columns(t)], proj[:, columns(t)], across_dims, preferred_element_type=F32
-    )
-    for d in range(1, ny):
-        tt = lax.rem(y - d + ny, ny) * 2 + c
-        ret = ret + lax.dot_general(
-            stream_ref[:, columns(tt)], proj[:, columns(tt)], across_dims,
-            preferred_element_type=F32,
-        )
-    for d in range(ny):
-        inner[d].wait_recv()
-        tt = lax.rem(y - d + ny, ny) * 2 + 1 - c
-        ret = ret + lax.dot_general(
-            stream_ref[:, columns(tt)], proj[:, columns(tt)], across_dims,
-            preferred_element_type=F32,
-        )
-    o_ref[...] = ret.astype(BF16)
-
     def expand(rows, width, depth):
         lane = lax.div(lax.broadcasted_iota(jnp.int32, (rows[0].shape[0], width), 1), depth)
         out = jnp.zeros((rows[0].shape[0], width), F32)
@@ -451,49 +478,6 @@
     state_row = lax.div(lax.broadcasted_iota(jnp.int32, (key_width, value_width), 0), key_dim)
     state_lane = lax.div(lax.broadcasted_iota(jnp.int32, (key_width, value_width), 1), value_dim)
     diagonal = state_row == state_lane
-    injected = lax.dot_general(
-        (query_ref[...].astype(F32) * grown).astype(BF16), o_ref[...], along_dims,
-        preferred_element_type=F32,
-    )
-    injected = jnp.where(diagonal, injected, 0.0)
-    folded = injected[:key_dim, :]
-    for h in range(1, heads):
-        folded = folded + injected[h * key_dim : (h + 1) * key_dim, :]
-    states[z] = folded.astype(BF16)
-    pair_copy = go(
-        remote(states.at[z], pair_state, u_send.at[0], u_recv.at[0], (z * 2 + 1 - x, t)),
-        "wait_send",
-    )
-    for i in range(1, nz):
-        go(
-            remote(
-                states.at[z], states.at[z], s_send.at[i], s_recv.at[z], (order[i] * 2 + x, t)
-            ),
-            "wait_send",
-        )
-
-    def piece(b, rows):
-        if wide % 128:
-            return blocks.at[b, rows]
-        return stream_ref.at[rows, pl.ds(pl.multiple_of(b * wide, wide), wide)]
-
-    if wide % 128:
-        for b in range(n):
-            blocks[b] = stream_ref[:, b * wide : (b + 1) * wide]
-
-    for i in range(nz):
-        for e in range(2):
-            if (i, e) != (0, 0):
-                to = member(i, e)
-                go(
-                    remote(
-                        piece(to, band(y, c)), cols_ref.at[s, band(y, c)],
-                        c_send.at[2 * i + e], c_recv.at[s], (to, t),
-                    ),
-                    "wait_send",
-                )
-    cols_ref[s] = piece(s, pl.ds(0, tokens))[...]
-
     for copy in ends_moving:
         copy.wait_recv()
     before = [jnp.zeros((1, value_width), F32)]
@@ -502,11 +486,20 @@
         ends = expand([ends_out[b, h : h + 1, 0:1] for h in range(heads)], value_width, value_dim)
         before.append(before[-1] + ends)
         since = since + ends * below(b, 2 * z + 2, 2 * n).astype(F32)
-    for b in range(n):
-        reach[b] = jnp.broadcast_to(
-            jnp.exp(jnp.minimum(before[b] - since, 0.0)) * below(2 * z + 1, b, 2 * n).astype(F32),
+    for zz in range(nz):
+        reach[zz] = jnp.broadcast_to(
+            jnp.exp(jnp.minimum(before[2 * zz] - since, 0.0))
+            * below(z, zz, nz).astype(F32),
             (8, value_width),
         )
+
+    def state_ends(b):
+        return expand(
+            [ends_out[b, h : h + 1, 0:1] for h in range(heads)], value_width, value_dim
+        )
+
+    lower = (1 - x).astype(F32)
+    half = key_dim // 2
 
     key_lane = lax.div(lax.broadcasted_iota(jnp.int32, (tokens, key_width), 1), key_dim)
     value_lane = lax.div(lax.broadcasted_iota(jnp.int32, (tokens, value_width), 1), value_dim)
@@ -521,94 +514,215 @@
         incoming[h * key_dim : (h + 1) * key_dim, :] = jnp.dot(
             incoming_ref[0, h].astype(BF16), put, preferred_element_type=F32
         ).astype(BF16)
+    for h in range(heads):
+        diff = head_total[h] - head_row[h]
+        fade[h] = jnp.where(first >= second, jnp.exp(jnp.minimum(diff, 0.0)), 0.0)
+        fade_turned[h] = jnp.where(first <= second, jnp.exp(jnp.minimum(-diff, 0.0)), 0.0)
+        pointed = lax.dot_general(
+            only(key_ref[...], key_lane, h), query_ref[...], across_dims,
+            preferred_element_type=F32,
+        )
+        score[h] = (pointed * fade_turned[h]).astype(BF16)
+    for d in range(1, ny):
+        outer[d].wait_recv()
+        theirs = stream_ref.at[:, columns(lax.rem(y - d + ny, ny) * 2 + c)]
+        inner[d] = go(
+            remote(theirs, theirs, h_send.at[d], h_recv.at[d], partner), "wait_send"
+        )
+    band_count = 2 * ny if tokens % (32 * ny) == 0 else 2
+    tall = tokens // band_count
+    wide = cols_ref.shape[2]
+    tp_bands = band_count > 2
+
+    def band(yy, cc):
+        return pl.ds(pl.multiple_of((yy * 2 + cc if tp_bands else cc) * tall, tall), tall)
+
+    ret = lax.dot_general(
+        stream_ref[:, columns(t)], proj[:, columns(t)], across_dims, preferred_element_type=F32
+    )
+    for d in range(1, ny):
+        tt = lax.rem(y - d + ny, ny) * 2 + c
+        ret = ret + lax.dot_general(
+            stream_ref[:, columns(tt)], proj[:, columns(tt)], across_dims,
+            preferred_element_type=F32,
+        )
+    for d in range(ny):
+        inner[d].wait_recv()
+
+    def piece(b, rows):
+        if wide % 128:
+            return blocks.at[b, rows]
+        return stream_ref.at[rows, pl.ds(pl.multiple_of(b * wide, wide), wide)]
+
+    if wide % 128:
+        for b in range(n):
+            blocks[b] = stream_ref[:, b * wide : (b + 1) * wide]
+
+    def send_columns(i, e):
+        to = member(i, e)
+        go(
+            remote(
+                piece(to, band(y, c)), cols_ref.at[s, band(y, c)],
+                c_send.at[2 * i + e], c_recv.at[s], (to, t),
+            ),
+            "wait_send",
+        )
+
+    for i, e in turns:
+        send_columns(i, e)
+    for d in range(ny):
+        tt = lax.rem(y - d + ny, ny) * 2 + 1 - c
+        ret = ret + lax.dot_general(
+            stream_ref[:, columns(tt)], proj[:, columns(tt)], across_dims,
+            preferred_element_type=F32,
+        )
+    o_ref[...] = ret.astype(BF16)
+
+    injected = lax.dot_general(
+        (query_ref[...].astype(F32) * grown).astype(BF16), o_ref[...], along_dims,
+        preferred_element_type=F32,
+    )
+    injected = jnp.where(diagonal, injected, 0.0)
+    folded = injected[:key_dim, :]
+    for h in range(1, heads):
+        folded = folded + injected[h * key_dim : (h + 1) * key_dim, :]
+    own_state[...] = folded.astype(BF16)
+    pair_copy = go(
+        remote(own_state, pair_state, u_send.at[0], u_recv.at[0], (z * 2 + 1 - x, t)),
+        "wait_send",
+    )
+    cols_ref[s] = piece(s, pl.ds(0, tokens))[...]
+
     query_grad = grown * lax.dot_general(
         o_ref[...], incoming[...], across_dims, preferred_element_type=F32
     )
     key_grad = jnp.zeros((tokens, key_width), F32)
     value_grad = jnp.zeros((tokens, value_width), F32)
-    for h in range(heads):
+    def head_grads(h, grads):
+        query_grad, key_grad, value_grad = grads
         o_head = only(o_ref[...], value_lane, h)
         v_head = only(value_ref[...], value_lane, h)
         q_head = only(query_ref[...], key_lane, h)
         k_head = only(key_ref[...], key_lane, h)
-        diff = head_total[h] - head_row[h]
-        fade = jnp.where(first >= second, jnp.exp(jnp.minimum(diff, 0.0)), 0.0)
-        fade_turned = jnp.where(first <= second, jnp.exp(jnp.minimum(-diff, 0.0)), 0.0)
         prob = lax.dot_general(o_head, value_ref[...], across_dims, preferred_element_type=F32)
         query_grad = query_grad + jnp.dot(
-            (prob * fade).astype(BF16), k_head, preferred_element_type=F32
+            (prob * fade[h]).astype(BF16), k_head, preferred_element_type=F32
         )
         prob = lax.dot_general(v_head, o_ref[...], across_dims, preferred_element_type=F32)
         key_grad = key_grad + jnp.dot(
-            (prob * fade_turned).astype(BF16), q_head, preferred_element_type=F32
-        )
-        score = lax.dot_general(k_head, query_ref[...], across_dims, preferred_element_type=F32)
-        value_grad = value_grad + jnp.dot(
-            (score * fade_turned).astype(BF16), o_head, preferred_element_type=F32
-        )
+            (prob * fade_turned[h]).astype(BF16), q_head, preferred_element_type=F32
+        )
+        value_grad = value_grad + jnp.dot(score[h], o_head, preferred_element_type=F32)
+        return query_grad, key_grad, value_grad
+
+    from_far, joined = {}, {}
+
+    def columns_arrive(i, e):
+        src, k = member(i, e), 2 * i + e
+        mine = cols_ref.at[src, band(y, c)]
+        remote(
+            piece(src, band(y, c)), mine, c_send.at[k], c_recv.at[src], (src, t)
+        ).wait_recv()
+        if tp_bands:
+            for d in range(1, ny):
+                from_far[d, k] = go(
+                    remote(mine, mine, v_send.at[d, k], v_recv.at[d, k], away(d)), "wait_send"
+                )
+        joined[0, k] = go(
+            remote(mine, mine, w_send.at[0, k], w_recv.at[0, k], partner), "wait_send"
+        )
+
+    grads = (query_grad, key_grad, value_grad)
+    for h in range(heads // 2):
+        grads = head_grads(h, grads)
+    pair_copy.wait_recv()
+    mine, other = own_state[...].astype(F32), pair_state[...].astype(F32)
+    both = lower * mine + (1.0 - lower) * other + jnp.exp(state_ends(z * 2)) * (
+        lower * other + (1.0 - lower) * mine
+    )
+    both_halves[0] = both[:half].astype(BF16)
+    both_halves[1] = both[half:].astype(BF16)
+    for i in range(1, nz):
+        go(
+            remote(
+                both_halves.at[x], states.at[z], s_send.at[i], s_recv.at[z], (order[i] * 2 + x, t)
+            ),
+            "wait_send",
+        )
+    for i, e in turns[:3]:
+        columns_arrive(i, e)
+    for h in range(heads // 2, heads):
+        grads = head_grads(h, grads)
+    query_grad, key_grad, value_grad = grads
     query_out[...] = query_grad.astype(BF16)
 
-    later = jnp.zeros((key_dim, value_width), F32)
+    def gather(i):
+        for e in range(2):
+            for d in range(ny if tp_bands else 1):
+                if (d, 2 * i + e) in joined:
+                    joined[d, 2 * i + e].wait_recv()
+        pair = pl.ds(order[i] * 2, 2)
+        added = lax.dot_general(
+            cols_ref[pair].reshape(2 * tokens, wide),
+            kept_out[pair].reshape(2 * tokens, kept_ref.shape[1]),
+            along_dims, preferred_element_type=F32,
+        )
+        if i == 0:
+            proj_grad[...] = added
+        else:
+            proj_grad[...] += added
+
+    for i, e in turns[3:5]:
+        columns_arrive(i, e)
+    later = jnp.zeros((half, value_width), F32)
     for i in range(1, nz):
         src = order[i]
         remote(
-            states.at[src], states.at[src], s_send.at[i], s_recv.at[src], (src * 2 + x, t)
+            both_halves.at[x], states.at[src], s_send.at[i], s_recv.at[src], (src * 2 + x, t)
         ).wait_recv()
-        later = later + reach[src * 2 + x][0:1, :] * states[src].astype(F32)
-    turn_out[...] = later.astype(BF16)
+        later = later + reach[src][0:1, :] * states[src].astype(F32)
+    later_halves[x] = later.astype(BF16)
     turned = go(
-        remote(turn_out, turn_in, u_send.at[1], u_recv.at[1], (z * 2 + 1 - x, t)), "wait_send"
-    )
-
-    from_far, from_partner = {}, {}
+        remote(
+            later_halves.at[x], later_halves.at[x], u_send.at[1], u_recv.at[1],
+            (z * 2 + 1 - x, t),
+        ),
+        "wait_send",
+    )
+    for i, e in turns[5:]:
+        columns_arrive(i, e)
+    for copy in kept_moving:
+        copy.wait_recv()
+    turned.wait_recv()
+    later = jnp.concatenate([later_halves[j].astype(F32) for j in range(2)], axis=0)
+    later = jnp.exp(lower * state_ends(z * 2 + 1)) * later + lower * pair_state[...].astype(F32)
+    stacked = jnp.concatenate([later.astype(BF16)] * heads, axis=0)
+    stacked = jnp.where(diagonal, stacked, jnp.zeros_like(stacked))
+    left = [end - own for end, own in zip(head_end, head_total)]
+    key_grad = key_grad + jnp.exp(expand(left, key_width, key_dim)) * lax.dot_general(
+        value_ref[...], stacked, across_dims, preferred_element_type=F32
+    )
+    key_out[...] = key_grad.astype(BF16)
+    value_grad = value_grad + jnp.exp(expand(left, value_width, value_dim)) * jnp.dot(
+        key_ref[...], stacked, preferred_element_type=F32
+    )
+    value_out[...] = value_grad.astype(BF16)
     for i in range(nz):
         for e in range(2):
             if (i, e) == (0, 0):
                 continue
             src, k = member(i, e), 2 * i + e
-            mine = cols_ref.at[src, band(y, c)]
-            remote(
-                piece(src, band(y, c)), mine, c_send.at[k], c_recv.at[src],
-                (src, t),
-            ).wait_recv()
             if tp_bands:
-                for d in range(1, ny):
-                    from_far[d, k] = go(
-                        remote(mine, mine, v_send.at[d, k], v_recv.at[d, k], away(d)),
-                        "wait_send",
-                    )
-            go(remote(mine, mine, w_send.at[0, k], w_recv.at[0, k], partner), "wait")
-    turned.wait_recv()
-    later = turn_out[...].astype(F32) + turn_in[...].astype(F32)
-    lower = (1 - x).astype(F32)
-    pair_ends = expand(
-        [ends_out[z * 2 + 1, h : h + 1, 0:1] for h in range(heads)], value_width, value_dim
-    )
-    pair_copy.wait_recv()
-    later = jnp.exp(lower * pair_ends) * later + lower * pair_state[...].astype(F32)
-    stacked = jnp.concatenate([later.astype(BF16)] * heads, axis=0)
-    stacked = jnp.where(diagonal, stacked, jnp.zeros_like(stacked))
-    left = [end - own for end, own in zip(head_end, head_total)]
-    key_grad = key_grad + jnp.exp(expand(left, key_width, key_dim)) * lax.dot_general(
-        value_ref[...], stacked, across_dims, preferred_element_type=F32
-    )
-    key_out[...] = key_grad.astype(BF16)
-    value_grad = value_grad + jnp.exp(expand(left, value_width, value_dim)) * jnp.dot(
-        key_ref[...], stacked, preferred_element_type=F32
-    )
-    value_out[...] = value_grad.astype(BF16)
-    if tp_bands:
-        for i in range(nz):
-            for e in range(2):
-                if (i, e) == (0, 0):
-                    continue
-                src, k = member(i, e), 2 * i + e
                 for d in range(1, ny):
                     from_far[d, k].wait_recv()
                     theirs = cols_ref.at[src, band(lax.rem(y - d + ny, ny), c)]
-                    go(
-                        remote(theirs, theirs, w_send.at[d, k], w_recv.at[d, k], partner), "wait"
+                    joined[d, k] = go(
+                        remote(theirs, theirs, w_send.at[d, k], w_recv.at[d, k], partner),
+                        "wait_send",
                     )
+        if i:
+            gather(i - 1)
+    gather(nz - 1)
     for wait in waits:
         wait()
 
@@ -623,12 +737,12 @@
     slots, model, width = n * cap, rows.shape[1], gate_w.shape[2]
     nz = n // 2
     state = (key.shape[1] // heads, value.shape[1])
+    half_state = (state[0] // 2, state[1])
     vmem = pl.BlockSpec(memory_space=pltpu.VMEM)
     return pl.pallas_call(
         functools.partial(main_kernel, n, ny, cap),
         out_shape=(
-            jax.ShapeDtypeStruct((n,) + kept.shape, BF16),
-            jax.ShapeDtypeStruct((n, tokens, model // n), BF16),
+            jax.ShapeDtypeStruct((model // n, kept.shape[1]), F32),
             jax.ShapeDtypeStruct(gate_w.shape, BF16),
             jax.ShapeDtypeStruct(up_w.shape, BF16),
             jax.ShapeDtypeStruct(down_w.shape, BF16),
@@ -637,19 +751,25 @@
             jax.ShapeDtypeStruct(value.shape, BF16),
         ),
         in_specs=[pl.BlockSpec(memory_space=pltpu.HBM)] * 14,
-        out_specs=[vmem] * 8,
+        out_specs=[vmem] * 7,
         scratch_shapes=[
+            pltpu.VMEM((n,) + kept.shape, BF16),
+            pltpu.VMEM((n, tokens, model // n), BF16),
             pltpu.VMEM((tokens, model), BF16),
             pltpu.VMEM((n, 8, 128), F32),
             pltpu.VMEM(proj.shape, BF16),
             pltpu.VMEM((key.shape[1], value.shape[1]), BF16),
             pltpu.VMEM((tokens, value.shape[1]), BF16),
-            pltpu.VMEM((nz,) + state, BF16),
-            pltpu.VMEM(state, BF16),
-            pltpu.VMEM((n, 8, value.shape[1]), F32),
+            pltpu.VMEM((nz,) + half_state, BF16),
             pltpu.VMEM(state, BF16),
             pltpu.VMEM(state, BF16),
+            pltpu.VMEM((nz, 8, value.shape[1]), F32),
+            pltpu.VMEM((2,) + half_state, BF16),
+            pltpu.VMEM((2,) + half_state, BF16),
             pltpu.VMEM((n, tokens, model // n) if model // n % 128 else (1, 8, 128), BF16),
+            pltpu.VMEM((heads, tokens, tokens), F32),
+            pltpu.VMEM((heads, tokens, tokens), F32),
+            pltpu.VMEM((heads, tokens, tokens), BF16),
             pltpu.VMEM(ids.shape, jnp.int32),
             pltpu.VMEM(weights.shape, F32),
             pltpu.VMEM(decay.shape, F32),
@@ -678,7 +798,7 @@
         ]
         + [dma((n,))] * 4
         + [dma((ny, n))] * 4
-        + [dma((ny, nz))] * 4
+        + [dma((ny, nz + 1))] * 4
         + [dma((n,))] * 2
         + [dma((ny,))] * 4
         + [dma((n,))] * 6
@@ -700,37 +820,27 @@
     )
 
 
-def final_kernel(cols_ref, kept_ref, *refs):
+def final_kernel(*refs):
     moved = len(refs) // 2
-    sources, proj_grad, targets, sems = (
-        refs[:moved - 1], refs[moved - 1], refs[moved:-1], refs[-1]
-    )
     copies = [
-        pltpu.make_async_copy(source, target, sems.at[j])
-        for j, (source, target) in enumerate(zip(sources, targets))
+        pltpu.make_async_copy(source, target, refs[-1].at[j])
+        for j, (source, target) in enumerate(zip(refs[:moved], refs[moved:-1]))
     ]
     for copy in copies:
         copy.start()
-    rows = cols_ref.shape[0] * cols_ref.shape[1]
-    proj_grad[...] = lax.dot_general(
-        cols_ref[...].reshape(rows, -1), kept_ref[...].reshape(rows, -1),
-        (((0,), (0,)), ((), ())), preferred_element_type=F32,
-    )
     for copy in copies:
         copy.wait()
 
 
-def final_part(cols, kept, *moved):
-    vmem = pl.BlockSpec(memory_space=pltpu.VMEM)
+def final_part(*moved):
     return pl.pallas_call(
         final_kernel,
-        out_shape=(jax.ShapeDtypeStruct((cols.shape[2], kept.shape[2]), F32),)
-        + tuple(jax.ShapeDtypeStruct(array.shape, array.dtype) for array in moved),
-        in_specs=[vmem] * (2 + len(moved)),
-        out_specs=[vmem] + [pl.BlockSpec(memory_space=pltpu.HBM)] * len(moved),
+        out_shape=tuple(jax.ShapeDtypeStruct(array.shape, array.dtype) for array in moved),
+        in_specs=[pl.BlockSpec(memory_space=pltpu.VMEM)] * len(moved),
+        out_specs=[pl.BlockSpec(memory_space=pltpu.HBM)] * len(moved),
         scratch_shapes=[pltpu.SemaphoreType.DMA((len(moved),))],
         compiler_params=pltpu.CompilerParams(vmem_limit_bytes=LIMIT // 4),
-    )(cols, kept, *moved)
+    )(*moved)
 
 
 def on_device(
@@ -752,12 +862,11 @@
     n, ny = lax.axis_size("sp"), lax.axis_size("tp") // 2
     tokens_here = moe_input.shape[0]
     capacity = -(-(5 * tokens_here // (2 * n)) // 16) * 16
-    kept_all, cols, *moved = main_part(
-        n, ny, capacity, expert_ids.T, expert_weights.T, log_decay.T, moe_input, out_grad,
-        retained, w_gate, w_up, w_down, out_proj, queries, keys, values, incoming_state,
-    )
     proj_grad, gate_grad, up_grad, down_grad, query_grad, key_grad, value_grad = final_part(
-        cols, kept_all, *moved
+        *main_part(
+            n, ny, capacity, expert_ids.T, expert_weights.T, log_decay.T, moe_input, out_grad,
+            retained, w_gate, w_up, w_down, out_proj, queries, keys, values, incoming_state,
+        )
     )
     return gate_grad, up_grad, down_grad, proj_grad, query_grad, key_grad, value_grad
 

time: 93 us -> 84.4 us (0.908)
  Pallas kernels: 92.1 us -> 83.4 us
    pallas_call x1, Pallas kernels: 88.4 us -> 80.5 us  [main_part(): pl.pallas_call(functools.partial(main_kernel, n, ny, cap), out_shape=(jax...]
where the time goes in v3:
time: 84.4 us; the launch traced here: 84.2 us
  Pallas kernels  83.4 us (99%)
    pallas_call x1, Pallas kernels, main_part(): pl.pallas_call(functools.partial(main_kernel, n, ny, cap), out_shape=(jax...  80.5 us
    pallas_call x1, Pallas kernels, final_part(): pl.pallas_call(final_kernel, out_shape=tuple((jax.ShapeDtypeStruct(array....  2.93 us

profile of v3, /device:TPU:0, one launch (start us, length us, event | category | flops | bytes accessed | tf_op | source)
XLA Modules:
  0.0 84.2 jit_solution(12056639637483924760)
XLA Ops:
  0.6 80.5 %shard_map.189 = (f32[256,384]{1,0:T(8,128)S(1)}, bf16[1,2048,512]{2,1,0:T(8,128)(2,1)S(1)}, bf16[1,2048,512]{2,1,0:T(8,128)(2,1)S(1)}, bf16[1,512,2048]{2,1,0:T...) custom-call(s32[2,192]{1,0:T(2,128)} %bitcast.4, ...), custom_call_target="tpu_custom_call" | custom-call | tf_op jit(solution)/shard_map/pallas_call | solution.py:742
  81.1 2.9 %shard_map.190 = (f32[256,384]{1,0:T(8,128)}, bf16[1,2048,512]{2,1,0:T(8,128)(2,1)}, bf16[1,2048,512]{2,1,0:T(8,128)(2,1)}, bf16[1,512,2048]{2,1,0:T(8,128)(2,1)...) custom-call(f32[256,384]{1,0:T(8,128)S(1)} %get-tuple-element.21.refs_0_, ...), custom_call_target="tpu_custom_call" | custom-call | tf_op jit(solution)/shard_map/pallas_call | solution.py:836

commit v4 on v3

--- a/solution.py
+++ b/solution.py
@@ -59,8 +59,8 @@
     n, ny, cap, ids_hbm, weights_hbm, decay_hbm, rows_hbm, grad_hbm, kept_hbm,
     gate_hbm, up_hbm, down_hbm, proj_hbm, query_hbm, key_hbm, value_hbm, incoming_hbm,
     proj_grad, gate_grad_ref, up_grad_ref, down_grad_ref, query_out, key_out, value_out,
-    kept_out, cols_ref, stream_ref, ends_out, proj, incoming, o_ref, states, own_state, pair_state, reach, both_halves,
-    later_halves,
+    kept_out, cols_ref, stream_ref, ends_out, proj, incoming, o_ref, states, own_state, pair_state, reach, both_state,
+
     blocks, fade, fade_turned, score, ids_ref, weights_ref, decay_ref, grad_ref, kept_ref, query_ref, key_ref, value_ref,
     incoming_ref, rows_v, gate_w, up_w, down_w, pick, send, slots, act, both_grads, part, near, pairs, far,
     share, back,
@@ -118,7 +118,7 @@
     ]
     for copy in loads:
         copy.start()
-    for copy in loads[:6]:
+    for copy in loads[:3]:
         copy.wait()
 
     ids = ids_ref[...].astype(F32)
@@ -145,6 +145,8 @@
     ends_out[s, pl.ds(0, heads), :] = jnp.broadcast_to(
         jnp.sum(decay_ref[...], axis=1, keepdims=True), (heads, 128)
     )
+    for copy in loads[3:5]:
+        copy.wait()
     cotangent = jnp.dot(picker, grad_ref[...], preferred_element_type=F32) * slot_weight
     send[:, 1] = cotangent.astype(BF16).reshape(n, cap, q)
     picked = jnp.dot(picker, rows_v[...], preferred_element_type=F32).astype(BF16)
@@ -212,15 +214,17 @@
         if j <= right_steps:
             moving["right"].wait_recv()
             held = at(z - j)
-            if j < right_steps:
-                moving["right"] = hop(j, 1, r_send, r_recv, kept_out.at[held])
             across(held, 2 * j - 1, kept_out.at[held])
         if j <= left_steps:
             moving["left"].wait_recv()
             held = at(z + j)
-            if j < left_steps:
-                moving["left"] = hop(j, -1, l_send, l_recv, kept_out.at[held])
             across(held, 2 * j, kept_out.at[held])
+
+    def kept_onward(j):
+        if j < right_steps:
+            moving["right"] = hop(j, 1, r_send, r_recv, kept_out.at[at(z - j)])
+        if j < left_steps:
+            moving["left"] = hop(j, -1, l_send, l_recv, kept_out.at[at(z + j)])
 
     from_far, from_partner = {}, {}
 
@@ -383,7 +387,7 @@
             )
         )
     def loaded():
-        for copy in loads[6:]:
+        for copy in loads[5:]:
             copy.wait()
 
     def forward(i):
@@ -421,8 +425,8 @@
             send_back(i - 2)
     arrive(last, 0)
     forward(last - 1)
+    arrive(last, 1)
     send_pairs(last - 2)
-    arrive(last, 1)
     kept_start()
     work(last - 1)
     if last > 2:
@@ -434,8 +438,8 @@
     relay(last, 1)
     send_pairs(last)
     kept_relay(1)
+    send_back(last - 1)
     work(last + 1)
-    send_back(last - 1)
     send_pairs(last + 1)
     send_back(last)
     down_grads()
@@ -449,11 +453,10 @@
     outer = {}
     for d in range(1, ny):
         outer[d] = go(remote(mine, mine, g_send.at[d], g_recv.at[d], away(d)), "wait_send")
+    kept_onward(1)
     inner = {}
     inner[0] = go(remote(mine, mine, h_send.at[0], h_recv.at[0], partner), "wait_send")
     in_grads(2, 4)
-    for j in range(2, nz):
-        kept_relay(j)
     value_dim, key_dim = value_ref.shape[1] // heads, key_ref.shape[1] // heads
     def expand(rows, width, depth):
         lane = lax.div(lax.broadcasted_iota(jnp.int32, (rows[0].shape[0], width), 1), depth)
@@ -499,7 +502,6 @@
         )
 
     lower = (1 - x).astype(F32)
-    half = key_dim // 2
 
     key_lane = lax.div(lax.broadcasted_iota(jnp.int32, (tokens, key_width), 1), key_dim)
     value_lane = lax.div(lax.broadcasted_iota(jnp.int32, (tokens, value_width), 1), value_dim)
@@ -632,20 +634,31 @@
             remote(mine, mine, w_send.at[0, k], w_recv.at[0, k], partner), "wait_send"
         )
 
+    def columns_relay(i, e):
+        src, k = member(i, e), 2 * i + e
+        for d in range(1, ny if tp_bands else 1):
+            from_far[d, k].wait_recv()
+            theirs = cols_ref.at[src, band(lax.rem(y - d + ny, ny), c)]
+            joined[d, k] = go(
+                remote(theirs, theirs, w_send.at[d, k], w_recv.at[d, k], partner), "wait_send"
+            )
+
     grads = (query_grad, key_grad, value_grad)
     for h in range(heads // 2):
         grads = head_grads(h, grads)
     pair_copy.wait_recv()
+    for j in range(2, nz):
+        kept_relay(j)
+        kept_onward(j)
     mine, other = own_state[...].astype(F32), pair_state[...].astype(F32)
     both = lower * mine + (1.0 - lower) * other + jnp.exp(state_ends(z * 2)) * (
         lower * other + (1.0 - lower) * mine
     )
-    both_halves[0] = both[:half].astype(BF16)
-    both_halves[1] = both[half:].astype(BF16)
+    both_state[...] = both.astype(BF16)
     for i in range(1, nz):
         go(
             remote(
-                both_halves.at[x], states.at[z], s_send.at[i], s_recv.at[z], (order[i] * 2 + x, t)
+                both_state, states.at[z], s_send.at[i], s_recv.at[z], (order[i] * 2 + x, t)
             ),
             "wait_send",
         )
@@ -672,29 +685,19 @@
         else:
             proj_grad[...] += added
 
-    for i, e in turns[3:5]:
+    for i, e in turns[3:]:
         columns_arrive(i, e)
-    later = jnp.zeros((half, value_width), F32)
+    for i, e in turns[:3]:
+        columns_relay(i, e)
+    later = jnp.zeros((key_dim, value_width), F32)
     for i in range(1, nz):
         src = order[i]
         remote(
-            both_halves.at[x], states.at[src], s_send.at[i], s_recv.at[src], (src * 2 + x, t)
+            both_state, states.at[src], s_send.at[i], s_recv.at[src], (src * 2 + x, t)
         ).wait_recv()
         later = later + reach[src][0:1, :] * states[src].astype(F32)
-    later_halves[x] = later.astype(BF16)
-    turned = go(
-        remote(
-            later_halves.at[x], later_halves.at[x], u_send.at[1], u_recv.at[1],
-            (z * 2 + 1 - x, t),
-        ),
-        "wait_send",
-    )
-    for i, e in turns[5:]:
-        columns_arrive(i, e)
     for copy in kept_moving:
         copy.wait_recv()
-    turned.wait_recv()
-    later = jnp.concatenate([later_halves[j].astype(F32) for j in range(2)], axis=0)
     later = jnp.exp(lower * state_ends(z * 2 + 1)) * later + lower * pair_state[...].astype(F32)
     stacked = jnp.concatenate([later.astype(BF16)] * heads, axis=0)
     stacked = jnp.where(diagonal, stacked, jnp.zeros_like(stacked))
@@ -707,21 +710,10 @@
         key_ref[...], stacked, preferred_element_type=F32
     )
     value_out[...] = value_grad.astype(BF16)
-    for i in range(nz):
-        for e in range(2):
-            if (i, e) == (0, 0):
-                continue
-            src, k = member(i, e), 2 * i + e
-            if tp_bands:
-                for d in range(1, ny):
-                    from_far[d, k].wait_recv()
-                    theirs = cols_ref.at[src, band(lax.rem(y - d + ny, ny), c)]
-                    joined[d, k] = go(
-                        remote(theirs, theirs, w_send.at[d, k], w_recv.at[d, k], partner),
-                        "wait_send",
-                    )
-        if i:
-            gather(i - 1)
+    for i, e in turns[3:]:
+        columns_relay(i, e)
+    for i in range(nz - 1):
+        gather(i)
     gather(nz - 1)
     for wait in waits:
         wait()
@@ -737,7 +729,6 @@
     slots, model, width = n * cap, rows.shape[1], gate_w.shape[2]
     nz = n // 2
     state = (key.shape[1] // heads, value.shape[1])
-    half_state = (state[0] // 2, state[1])
     vmem = pl.BlockSpec(memory_space=pltpu.VMEM)
     return pl.pallas_call(
         functools.partial(main_kernel, n, ny, cap),
@@ -760,12 +751,11 @@
             pltpu.VMEM(proj.shape, BF16),
             pltpu.VMEM((key.shape[1], value.shape[1]), BF16),
             pltpu.VMEM((tokens, value.shape[1]), BF16),
-            pltpu.VMEM((nz,) + half_state, BF16),
+            pltpu.VMEM((nz,) + state, BF16),
             pltpu.VMEM(state, BF16),
             pltpu.VMEM(state, BF16),
             pltpu.VMEM((nz, 8, value.shape[1]), F32),
-            pltpu.VMEM((2,) + half_state, BF16),
-            pltpu.VMEM((2,) + half_state, BF16),
+            pltpu.VMEM(state, BF16),
             pltpu.VMEM((n, tokens, model // n) if model // n % 128 else (1, 8, 128), BF16),
             pltpu.VMEM((heads, tokens, tokens), F32),
             pltpu.VMEM((heads, tokens, tokens), F32),
@@ -803,7 +793,7 @@
         + [dma((ny,))] * 4
         + [dma((n,))] * 6
         + [dma((nz,))] * 2
-        + [dma((2,))] * 2
+        + [dma((1,))] * 2
         + [dma((n,))] * 2
         + [dma((ny, n))] * 4,
         compiler_params=pltpu.CompilerParams(

time: 84.4 us -> 79.2 us (0.938)
  Pallas kernels: 83.4 us -> 78.3 us
    pallas_call x1, Pallas kernels: 80.5 us -> 75.3 us  [main_part(): pl.pallas_call(functools.partial(main_kernel, n, ny, cap), out_shape=(jax...]
where the time goes in v4:
time: 79.2 us; the launch traced here: 79.1 us
  Pallas kernels  78.3 us (99%)
  between operations  0.81 us (1%)
    pallas_call x1, Pallas kernels, main_part(): pl.pallas_call(functools.partial(main_kernel, n, ny, cap), out_shape=(jax...  75.3 us
    pallas_call x1, Pallas kernels, final_part(): pl.pallas_call(final_kernel, out_shape=tuple((jax.ShapeDtypeStruct(array....  2.93 us

profile of v4, /device:TPU:0, one launch (start us, length us, event | category | flops | bytes accessed | tf_op | source)
XLA Modules:
  0.0 79.1 jit_solution(7132604486900225728)
XLA Ops:
  0.6 75.3 %shard_map.189 = (f32[256,384]{1,0:T(8,128)S(1)}, bf16[1,2048,512]{2,1,0:T(8,128)(2,1)S(1)}, bf16[1,2048,512]{2,1,0:T(8,128)(2,1)S(1)}, bf16[1,512,2048]{2,1,0:T...) custom-call(s32[2,192]{1,0:T(2,128)} %bitcast.4, ...), custom_call_target="tpu_custom_call" | custom-call | tf_op jit(solution)/shard_map/pallas_call | solution.py:733
  76.0 2.9 %shard_map.190 = (f32[256,384]{1,0:T(8,128)}, bf16[1,2048,512]{2,1,0:T(8,128)(2,1)}, bf16[1,2048,512]{2,1,0:T(8,128)(2,1)}, bf16[1,512,2048]{2,1,0:T(8,128)(2,1)...) custom-call(f32[256,384]{1,0:T(8,128)S(1)} %get-tuple-element.21.refs_0_, ...), custom_call_target="tpu_custom_call" | custom-call | tf_op jit(solution)/shard_map/pallas_call | solution.py:826

commit v5 on v4

--- a/solution.py
+++ b/solution.py
@@ -689,6 +689,9 @@
         columns_arrive(i, e)
     for i, e in turns[:3]:
         columns_relay(i, e)
+    for copy in kept_moving:
+        copy.wait_recv()
+    gather(0)
     later = jnp.zeros((key_dim, value_width), F32)
     for i in range(1, nz):
         src = order[i]
@@ -696,8 +699,6 @@
             both_state, states.at[src], s_send.at[i], s_recv.at[src], (src * 2 + x, t)
         ).wait_recv()
         later = later + reach[src][0:1, :] * states[src].astype(F32)
-    for copy in kept_moving:
-        copy.wait_recv()
     later = jnp.exp(lower * state_ends(z * 2 + 1)) * later + lower * pair_state[...].astype(F32)
     stacked = jnp.concatenate([later.astype(BF16)] * heads, axis=0)
     stacked = jnp.where(diagonal, stacked, jnp.zeros_like(stacked))
@@ -712,7 +713,7 @@
     value_out[...] = value_grad.astype(BF16)
     for i, e in turns[3:]:
         columns_relay(i, e)
-    for i in range(nz - 1):
+    for i in range(1, nz - 1):
         gather(i)
     gather(nz - 1)
     for wait in waits:

time: 79.2 us -> 79.5 us (level)
  no operation moved by 1% of the time
where the time goes in v5:
time: 79.5 us; the launch traced here: 79.4 us
  Pallas kernels  78.6 us (99%)
  between operations  0.81 us (1%)
    pallas_call x1, Pallas kernels, main_part(): pl.pallas_call(functools.partial(main_kernel, n, ny, cap), out_shape=(jax...  75.6 us
    pallas_call x1, Pallas kernels, final_part(): pl.pallas_call(final_kernel, out_shape=tuple((jax.ShapeDtypeStruct(array....  2.93 us

profile of v5, /device:TPU:0, one launch (start us, length us, event | category | flops | bytes accessed | tf_op | source)
XLA Modules:
  0.0 79.4 jit_solution(12863484408626183920)
XLA Ops:
  0.6 75.6 %shard_map.189 = (f32[256,384]{1,0:T(8,128)S(1)}, bf16[1,2048,512]{2,1,0:T(8,128)(2,1)S(1)}, bf16[1,2048,512]{2,1,0:T(8,128)(2,1)S(1)}, bf16[1,512,2048]{2,1,0:T...) custom-call(s32[2,192]{1,0:T(2,128)} %bitcast.4, ...), custom_call_target="tpu_custom_call" | custom-call | tf_op jit(solution)/shard_map/pallas_call | solution.py:734
  76.3 2.9 %shard_map.190 = (f32[256,384]{1,0:T(8,128)}, bf16[1,2048,512]{2,1,0:T(8,128)(2,1)}, bf16[1,2048,512]{2,1,0:T(8,128)(2,1)}, bf16[1,512,2048]{2,1,0:T(8,128)(2,1)...) custom-call(f32[256,384]{1,0:T(8,128)S(1)} %get-tuple-element.21.refs_0_, ...), custom_call_target="tpu_custom_call" | custom-call | tf_op jit(solution)/shard_map/pallas_call | solution.py:827
